TPU v7x, 256 devices: a whole 4x4x8 slice. The times are simulated.
256 devices in a mesh: sp: 16 (over y, x), dp: 16 (over z, core).
Axes of the slice: x: 4, y: 4, z: 8, core: 2. Of those that a mesh axis runs over, the one named last changes fastest.
Arguments:
- tokens: bfloat16 [16, 4096, 2048], P('dp', 'sp'), may hold values from -6 to 6
- key_weight: bfloat16 [2048, 2048], P('dp'), may hold values from -0.125 to 0.125
- queries: bfloat16 [16, 4096, 16, 128], P('dp', None, 'sp'), may hold values from -1.5 to 1.5
- values: bfloat16 [16, 4096, 16, 256], P('dp', None, 'sp'), may hold values from -1.5 to 1.5
- cotangent: bfloat16 [16, 4096, 4096], P('dp', 'sp'), may hold values from -6 to 6
- log_decay: float32 [16], replicated, may hold values from -0.034 to 0, as said below
Outputs:
- grad_tokens: bfloat16 [16, 4096, 2048], P('dp', 'sp')
- grad_queries: bfloat16 [16, 4096, 16, 128], P('dp', None, 'sp')
- grad_values: bfloat16 [16, 4096, 16, 256], P('dp', None, 'sp')
- grad_key_weight: float32 [2048, 2048], P('dp')
Inputs may be any that keep to these rules, and one draw needn't show every extreme that they name: `log_decay`: every entry is below zero.
All inputs are finite; a program needn't handle non-finite values.
Results may differ from a plain program's by a relative error of at most 0.0075.
Values may be sent and summed in bfloat16 or wider, within the bound.
A program may use at most 128 MiB of HBM per device.

v0:
```python
import jax
import jax.numpy as jnp
from jax import lax
from jax.sharding import PartitionSpec as P

BLOCK = 128


def product(form, left, right):
    return jnp.einsum(form, left, right, preferred_element_type=jnp.float32)


def rotation(seq_len, half):
    position = jnp.arange(seq_len, dtype=jnp.float32)
    frequency = 10000.0 ** (-jnp.arange(half, dtype=jnp.float32) / half)
    angle = position[:, None] * frequency[None, :]
    return (jnp.cos(angle)[:, None, :], jnp.sin(angle)[:, None, :])


def rotate(vectors, cosine, sine):
    half = vectors.shape[-1] // 2
    front, back = (vectors[..., :half], vectors[..., half:])
    return jnp.concatenate([front * cosine - back * sine, front * sine + back * cosine], axis=-1)


def unrotate(grads, cosine, sine):
    half = grads.shape[-1] // 2
    front, back = (grads[..., :half], grads[..., half:])
    return jnp.concatenate([front * cosine + back * sine, back * cosine - front * sine], axis=-1)


def retention_backward(query_rows, key_rows, value_rows, cotan_rows, head_decay):
    seq_len, heads_here, key_width = query_rows.shape
    nblocks = seq_len // BLOCK
    cosine, sine = rotation(seq_len, key_width // 2)
    factor = key_width ** (-0.5)
    rot_query = rotate(query_rows.astype(jnp.float32), cosine, sine).astype(jnp.bfloat16)
    rot_key = (rotate(key_rows.astype(jnp.float32), cosine, sine) * factor).astype(jnp.bfloat16)

    def blocks(array):
        return array.reshape(nblocks, BLOCK, heads_here, array.shape[-1])

    block_query, block_key = (blocks(rot_query), blocks(rot_key))
    block_value, block_cotan = (blocks(value_rows), blocks(cotan_rows))
    inside = jnp.arange(BLOCK, dtype=jnp.float32)
    offset = inside[:, None] - inside[None, :]
    within = jnp.where(
        offset[None] >= 0, jnp.exp(jnp.maximum(offset, 0.0)[None] * head_decay[:, None, None]), 0.0
    )
    rising = jnp.exp((inside + 1.0)[:, None] * head_decay[None, :])[None, :, :, None]
    falling = jnp.exp((BLOCK - 1.0 - inside)[:, None] * head_decay[None, :])[None, :, :, None]
    scores = (product("nihd,njhd->nhij", block_query, block_key) * within[None]).astype(
        jnp.bfloat16
    )
    mixing = (product("nihe,njhe->nhij", block_cotan, block_value) * within[None]).astype(
        jnp.bfloat16
    )
    decayed_queries = (block_query.astype(jnp.float32) * rising).astype(jnp.bfloat16)
    decayed_keys = (block_key.astype(jnp.float32) * falling).astype(jnp.bfloat16)
    block_states = product("nihd,nihe->nhde", decayed_keys, block_value)
    block_trails = product("nihd,nihe->nhde", decayed_queries, block_cotan)
    block_index = jnp.arange(nblocks, dtype=jnp.float32)
    spacing = block_index[:, None] - block_index[None, :] - 1.0
    earlier = jnp.where(
        spacing[None] >= 0,
        jnp.exp(jnp.maximum(spacing, 0.0)[None] * BLOCK * head_decay[:, None, None]),
        0.0,
    )
    later = jnp.transpose(earlier, (0, 2, 1))
    entering = jnp.einsum(
        "hnm,mhde->nhde", earlier, block_states, precision=lax.Precision.HIGHEST
    ).astype(jnp.bfloat16)
    trailing = jnp.einsum(
        "hnm,mhde->nhde", later, block_trails, precision=lax.Precision.HIGHEST
    ).astype(jnp.bfloat16)
    grad_rq = product("nhij,njhd->nihd", mixing, block_key) + rising * product(
        "nihe,nhde->nihd", block_cotan, entering
    )
    grad_rk = product("nhij,nihd->njhd", mixing, block_query) + falling * product(
        "nihe,nhde->nihd", block_value, trailing
    )
    grad_value = product("nhij,nihe->njhe", scores, block_cotan) + falling * product(
        "nihd,nhde->nihe", block_key, trailing
    )
    grad_rq = grad_rq.reshape(seq_len, heads_here, key_width)
    grad_rk = grad_rk.reshape(seq_len, heads_here, key_width)
    grad_query = unrotate(grad_rq, cosine, sine).astype(jnp.bfloat16)
    grad_key = (unrotate(grad_rk, cosine, sine) * factor).astype(jnp.bfloat16)
    grad_value = grad_value.reshape(seq_len, heads_here, -1).astype(jnp.bfloat16)
    return (grad_query, grad_key, grad_value)


def weight_terms(source, token_rows):
    return jnp.einsum("tq,td->qd", source, token_rows, preferred_element_type=jnp.float32)


def body(tokens, key_weight, queries, values, cotangent, log_decay):
    gathered = lax.all_gather(key_weight, "dp", axis=0, tiled=True)
    token_rows = tokens[0]
    key_proj = jnp.einsum(
        "td,qd->tq", token_rows, gathered, preferred_element_type=jnp.float32
    ).astype(jnp.bfloat16)
    head_keys, head_cotan = (
        lax.all_to_all(key_proj[None], "sp", split_axis=2, concat_axis=1, tiled=True),
        lax.all_to_all(cotangent, "sp", split_axis=2, concat_axis=1, tiled=True),
    )
    seq_len = head_keys.shape[1]
    heads_here = queries.shape[2]
    head_start = lax.axis_index("sp") * heads_here
    head_decay = lax.dynamic_slice_in_dim(log_decay, head_start, heads_here)
    grad_query, grad_key, grad_value = retention_backward(
        queries[0],
        head_keys[0].reshape(seq_len, heads_here, -1),
        values[0],
        head_cotan[0].reshape(seq_len, heads_here, -1),
        head_decay,
    )
    returned = lax.all_to_all(
        grad_key.reshape(1, seq_len, -1), "sp", split_axis=1, concat_axis=2, tiled=True
    )
    key_grads = returned[0]
    grad_tokens = jnp.dot(key_grads, gathered, preferred_element_type=jnp.float32).astype(
        jnp.bfloat16
    )
    owned = lax.psum_scatter(
        weight_terms(key_grads, token_rows), "dp", scatter_dimension=0, tiled=True
    )
    weight_grad = lax.psum(owned, "sp")
    return (grad_tokens[None], grad_query[None], grad_value[None], weight_grad)


def solution(mesh):
    return jax.shard_map(
        body,
        mesh=mesh,
        in_specs=(
            P("dp", "sp", None),
            P("dp", None),
            P("dp", None, "sp", None),
            P("dp", None, "sp", None),
            P("dp", "sp", None),
            P(),
        ),
        out_specs=(
            P("dp", "sp", None),
            P("dp", None, "sp", None),
            P("dp", None, "sp", None),
            P("dp", None),
        ),
        check_vma=False,
    )
```

profile of v0, /device:TPU:1, one launch (start us, length us, event | category | flops | bytes accessed | tf_op | source)
XLA Modules:
  0.0 448.4 jit_solution(4986535643848774581)
XLA Ops:
  7.9 10.0 %copy.55 = bf16[1,256,4096]{1,0,2:T(2,128)(2,1)} copy(bf16[1,256,4096]{2,1,0:T(8,128)(2,1)} %param.10) | data formatting | bytes 4194304 | tf_op args[4]
  18.5 22.9 %reduce = bf16[4096,256]{1,0:T(8,128)(2,1)} reduce(bf16[4096,1,256]{2,1,0:T(2,128)(2,1)} %bitcast.127, bf16[]{:T(256)} %broadcast.209), dimensions={1}, to_apply=%bitcast.88.reduce_sub_computation | reduce | bytes 4194306
  45.4 7.7 %all-to-all-start = ((bf16[16,2,32768]{2,1,0:T(2,128)(2,1)}), bf16[16,2,32768]{2,1,0:T(2,128)(2,1)}, u32[]{:S(2)}, u32[]{:S(2)}) async-start(bf16[16,2,32768]{2,1,0:T(2,128)(2,1)} %reshape.451), calls=%async_computation | async-start | bytes 4194304 | tf_op jit(solution)/shard_map/all_to_all | solution.py:105
  55.8 14.1 %all-gather.2.cloned.1.call-done = bf16[2048,2048]{1,0:T(8,128)(2,1)} async-done(((bf16[128,2048]{1,0:T(8,128)(2,1)}), bf16[2048,2048]{1,0:T(8,128)(2,1)}) %all-gather.2.cloned.1.call-update) | async-done | bytes 8388624 | tf_op jit(solution)/shard_map/all_gather | solution.py:98
  69.9 6.7 %fusion.6 = bf16[1,256,2048]{2,1,0:T(8,128)(2,1)} fusion(bf16[2048,2048]{1,0:T(8,128)(2,1)} %all-gather.2.cloned.1.call-done, bf16[1,256,2048]{2,1,0:T(8,128)(2,1)S(1)} %copy-done.11), kind=kOutput, calls=%fused_computation.10 | convolution fusion | flops 2148007936 | bytes 10485760 | tf_op jit(solution)/shard_map/td,qd->tq/dot_general | solution.py:100
  76.6 5.9 %copy.64 = bf16[1,256,2048]{1,0,2:T(2,128)(2,1)} copy(bf16[1,256,2048]{2,1,0:T(8,128)(2,1)} %fusion.6) | data formatting | bytes 2097152 | tf_op jit(solution)/shard_map/broadcast_in_dim | solution.py:104
  82.5 11.7 %reduce.1 = bf16[2048,256]{1,0:T(8,128)(2,1)S(1)} reduce(bf16[2048,1,256]{2,1,0:T(2,128)(2,1)} %bitcast.135, bf16[]{:T(256)} %broadcast.209), dimensions={1}, to_apply=%bitcast.92.reduce_sub_computation | reduce | bytes 2097154
  95.3 6.5 %all-to-all-start.2 = ((bf16[16,2,16384]{2,1,0:T(2,128)(2,1)}), bf16[16,2,16384]{2,1,0:T(2,128)(2,1)S(1)}, u32[]{:S(2)}, u32[]{:S(2)}) async-start(bf16[16,2,16384]{2,1,0:T(2,128)(2,1)} %reshape.455), calls=%async_computation.2 | async-start | bytes 2097152 | tf_op jit(solution)/shard_map/all_to_all | solution.py:104
  105.1 10.4 %reshape.452 = bf16[4096,1,256]{2,1,0:T(2,128)(2,1)} reshape(bf16[16,2,32768]{2,1,0:T(2,128)(2,1)} %all-to-all-done) | data formatting | bytes 4194304
  130.1 6.1 %copy.65 = f32[1,256,16,128]{3,1,2,0:T(8,128)} copy(bf16[1,256,16,128]{1,0,3,2:T(2,128)(2,1)} %bitcast.136) | data formatting | bytes 3145728 | tf_op jit(solution)/shard_map/convert_element_type | solution.py:38
  136.2 10.5 %multiply_subtract_fusion = (f32[4096,1,64]{2,0,1:T(8,128)S(1)}, f32[4096,1,64]{2,0,1:T(8,128)S(1)}, bf16[4096,1,64]{2,0,1:T(8,128)(2,1)S(1)}, bf16[4096,1,64]{2,0,1:T(8,128)(2,1)S(1)}) fusion(f32[4096,1,128]{2,0,1:T(8,128)} %bitcast.118, f32[64]{0:T(128)S(1)} %multiply_power_fusion, f32[4096,1,128]{2,0,1:T(8,128)} %bitcast_convert_fusion), kind=kLoop, calls=%fused_computation.27 | loop fusion | flops 3932160 | bytes 7340288 | tf_op jit(solution)/shard_map/sub | solution.py:23
  151.8 5.8 %convert_bitcast_fusion = bf16[32,128,256]{2,0,1:T(8,128)(2,1)S(1)} fusion(f32[32,128,256]{2,1,0:T(8,128)S(1)} %fusion.28, f32[]{:T(128)S(6)} %mul.332), kind=kOutput, calls=%fused_computation.24 | convolution fusion | flops 403707904 | bytes 6291460 | tf_op jit(solution)/shard_map/hnm,mhde->nhde/dot_general | solution.py:70
  157.6 5.9 %convert_bitcast_fusion.1 = bf16[32,128,256]{2,0,1:T(8,128)(2,1)S(1)} fusion(f32[32,128,256]{2,1,0:T(8,128)S(1)} %fusion.27, f32[]{:T(128)S(6)} %mul.332), kind=kOutput, calls=%fused_computation.30 | convolution fusion | flops 403707904 | bytes 6291460 | tf_op jit(solution)/shard_map/hnm,mhde->nhde/dot_general | solution.py:73
  166.7 9.7 %fusion.35 = (bf16[1,4096,1,64]{3,1,2,0:T(8,128)(2,1)}, bf16[1,4096,1,64]{3,1,2,0:T(8,128)(2,1)}, f32[4096,1,64]{2,0,1:T(8,128)S(1)}, f32[4096,1,64]{2,0,1:T(8,128)S(1)}) fusion(f32[4096,1,128]{2,0,1:T(8,128)S(1)} %bitcast.119, f32[64]{0:T(128)S(1)} %multiply_power_fusion, f32[4096,1,128]{2,0,1:T(8,128)S(1)} %bitcast.120), kind=kLoop, calls=%fused_computation.53 | loop fusion | flops 3932160 | bytes 7340288 | tf_op jit(solution)/shard_map/concatenate | solution.py:29
  176.4 5.1 %fusion.54 = bf16[4096,1,128]{2,1,0:T(2,128)(2,1)S(1)} fusion(f32[1,4096,64]{2,0,1:T(1,128)S(1)} %bitcast.133, f32[1,4096,64]{2,0,1:T(1,128)S(1)} %bitcast.134), kind=kLoop, calls=%fused_computation.77 | loop fusion | flops 1572864 | bytes 3145728
  181.5 23.6 %reduce.2 = bf16[4096,128]{1,0:T(8,128)(2,1)} reduce(bf16[4096,1,128]{2,1,0:T(2,128)(2,1)S(1)} %fusion.54, bf16[]{:T(256)} %broadcast.209), dimensions={1}, to_apply=%fusion.54.reduce_sub_computation | reduce | bytes 2097154
  206.5 22.8 %all_to_all.39 = bf16[16,2,16384]{2,1,0:T(2,128)(2,1)} all-to-all(bf16[16,2,16384]{2,1,0:T(2,128)(2,1)S(1)} %reshape.453), channel_id=1, replica_groups=mesh['sp'=16,'dp'=16] {'sp'}, dimensions={0} | all-to-all | bytes 2097152 | tf_op jit(solution)/shard_map/all_to_all | solution.py:118
  229.2 4.3 reshape.454
  236.3 8.1 %fusion.29 = f32[2048,2048]{1,0:T(8,128)} fusion(bf16[256,2048]{0,1:T(8,128)(2,1)S(1)} %bitcast.129, bf16[1,256,2048]{2,1,0:T(8,128)(2,1)S(1)} %copy-done.12), kind=kOutput, calls=%fused_computation.46 | convolution fusion | flops 2147483648 | bytes 18874368 | tf_op jit(solution)/shard_map/tq,td->qd/dot_general | solution.py:94
  246.0 5.0 %fusion.26 = f32[32,128,256]{2,1,0:T(8,128)} fusion(bf16[32,128,256]{2,1,0:T(8,128)(2,1)S(1)} %bitcast.117, bf16[32,128,128]{2,1,0:T(8,128)(2,1)S(1)} %fusion.8, f32[128,128]{1,0:T(8,128)S(1)} %exponential_select_fusion, bf16[32,128,64]{2,1,0:T(8,128)(2,1)} %bitcast.123, bf16[32,128,64]{2,1,0:T(8,128)(2,1)} %bitcast.126), kind=kOutput, calls=%fused_computation.41 | convolution fusion | flops 405798912 | bytes 8454144 | tf_op jit(solution)/shard_map/nhij,nihe->njhe/dot_general | solution.py:10
  254.8 85.4 %reduce-scatter.2.cloned.1.call-done = f32[128,2048]{1,0:T(8,128)} async-done(((f32[2048,2048]{1,0:T(8,128)}), f32[128,2048]{1,0:T(8,128)}) %reduce-scatter.2.cloned.1.call-update) | async-done | bytes 1048592 | tf_op jit(solution)/shard_map/reduce_scatter | solution.py:125
  340.2 5.3 %fusion = bf16[32,1,256,128]{2,3,0,1:T(8,128)(2,1)} fusion(f32[32,128,256]{2,1,0:T(8,128)} %fusion.26, bf16[32,128,128]{2,1,0:T(8,128)(2,1)S(1)} %fusion.8, f32[128]{0:T(128)S(1)} %get-tuple-element.17, bf16[32,128,256]{2,0,1:T(8,128)(2,1)S(1)} %copy-done.5), kind=kOutput, calls=%fused_computation.1 | convolution fusion | flops 271581184 | bytes 9437696 | tf_op jit(solution)/shard_map/nihd,nhde->nihe/dot_general | solution.py:10
  345.5 6.8 %fusion.5 = bf16[1,256,2048]{2,1,0:T(8,128)(2,1)} fusion(bf16[256,2048]{0,1:T(8,128)(2,1)S(1)} %bitcast.130, bf16[2048,2048]{1,0:T(8,128)(2,1)} %all-gather.2.cloned.1.call-done), kind=kOutput, calls=%fused_computation.9 | convolution fusion | flops 2148007936 | bytes 10485760 | tf_op jit(solution)/shard_map/dot_general | solution.py:122
  352.4 87.0 %all-reduce.2.cloned.1.call-done = f32[128,2048]{1,0:T(8,128)} async-done(((f32[128,2048]{1,0:T(8,128)}), f32[128,2048]{1,0:T(8,128)}) %all-reduce.2.cloned.1.call-update) | async-done | bytes 1048592 | tf_op jit(solution)/shard_map/psum | solution.py:128
  (60 shorter events, 46.1 us)
Async XLA Ops:
  7.2 116.2 %copy-start = (bf16[1,4096,1,256]{3,1,2,0:T(8,128)(2,1)S(1)}, bf16[1,4096,1,256]{3,1,2,0:T(8,128)(2,1)}, u32[]{:S(2)}) copy-start(bf16[1,4096,1,256]{3,1,2,0:T(8,128)(2,1)} %param.9) | copy-start | bytes 6291460
  7.2 62.7 %all-gather.2.cloned.1.call-start = ((), (), s32[]{:S(2)}) async-start(), calls=%async_computation.4 | async-start | bytes 8912896 | tf_op jit(solution)/shard_map/all_gather | solution.py:98
  45.4 7.7 %copy-start.13 = (f32[16]{0:T(128)S(1)}, f32[16]{0:T(128)}, u32[]{:S(2)}) copy-start(f32[16]{0:T(128)} %param.11) | copy-start | bytes 196
  45.4 24.5 %copy-start.11 = (bf16[1,256,2048]{2,1,0:T(8,128)(2,1)S(1)}, bf16[1,256,2048]{2,1,0:T(8,128)(2,1)}, u32[]{:S(2)}) copy-start(bf16[1,256,2048]{2,1,0:T(8,128)(2,1)} %param.6) | copy-start | bytes 3145732
  45.4 49.9 %all-to-all-start = ((bf16[16,2,32768]{2,1,0:T(2,128)(2,1)}), bf16[16,2,32768]{2,1,0:T(2,128)(2,1)}, u32[]{:S(2)}, u32[]{:S(2)}) async-start(bf16[16,2,32768]{2,1,0:T(2,128)(2,1)} %reshape.451), calls=%async_computation | async-start | bytes 4194304 | tf_op jit(solution)/shard_map/all_to_all | solution.py:105
  95.3 31.3 %all-to-all-start.2 = ((bf16[16,2,16384]{2,1,0:T(2,128)(2,1)}), bf16[16,2,16384]{2,1,0:T(2,128)(2,1)S(1)}, u32[]{:S(2)}, u32[]{:S(2)}) async-start(bf16[16,2,16384]{2,1,0:T(2,128)(2,1)} %reshape.455), calls=%async_computation.2 | async-start | bytes 2097152 | tf_op jit(solution)/shard_map/all_to_all | solution.py:104
  101.9 238.3 %reduce-scatter.2.cloned.1.call-start = ((), (), s32[]{:S(2)}) async-start(), calls=%async_computation.5 | async-start | bytes 17825792 | tf_op jit(solution)/shard_map/reduce_scatter | solution.py:125
  146.7 3.3 copy-start.6
  146.7 3.3 copy-start.7
  147.3 1.3 copy-start.10
  149.1 1.6 copy-start.2
  163.5 1.6 copy-start.4
  234.7 1.6 copy-start.12
  236.3 8.1 %copy-start.8 = (bf16[1,256,16,128]{1,3,2,0:T(8,128)(2,1)}, bf16[1,256,16,128]{1,3,2,0:T(8,128)(2,1)S(1)}, u32[]{:S(2)}) copy-start(bf16[1,256,16,128]{1,3,2,0:T(8,128)(2,1)S(1)} %copy.63) | copy-start | bytes 3145732
  244.4 1.6 copy-start.3
  244.4 194.9 %all-reduce.2.cloned.1.call-start = ((), (), s32[]{:S(2)}) async-start(), calls=%async_computation.6 | async-start | bytes 2097152 | tf_op jit(solution)/shard_map/psum | solution.py:128
  251.0 89.2 %copy-start.5 = (bf16[32,128,256]{2,0,1:T(8,128)(2,1)S(1)}, bf16[32,128,256]{2,0,1:T(8,128)(2,1)}, u32[]{:S(2)}) copy-start(bf16[32,128,256]{2,0,1:T(8,128)(2,1)} %copy-done.4) | copy-start | bytes 6291460
  340.2 5.3 %copy-start.9 = (bf16[1,256,16,128]{1,3,2,0:T(8,128)(2,1)S(1)}, bf16[1,256,16,128]{1,3,2,0:T(8,128)(2,1)}, u32[]{:S(2)}) copy-start(bf16[1,256,16,128]{1,3,2,0:T(8,128)(2,1)} %copy-done.8) | copy-start | bytes 3145732
  345.5 96.1 %copy-start.1 = (bf16[1,4096,1,256]{3,1,2,0:T(8,128)(2,1)S(1)}, bf16[1,4096,1,256]{3,1,2,0:T(8,128)(2,1)}, u32[]{:S(2)}) copy-start(bf16[1,4096,1,256]{3,1,2,0:T(8,128)(2,1)} %param.9) | copy-start | bytes 6291460
Sparse Core Ops, SparseCore 0:
  9.8 60.0 all-gather.1
  244.5 95.6 reduce-scatter.1
  343.4 95.8 all-reduce.1
where the time goes:
time: 457 us; the launch traced here: 448 us
  waiting for transfers between devices  187 us (41%)
  other arithmetic  92 us (20%)
  local copies, waits for them, and re-layouts  63 us (14%)
  matrix products  53.4 us (12%)
  blocking collectives  22.8 us (5%)
  starting transfers between devices  15.2 us (3%)
  between operations  14.9 us (3%)
    psum x1, waiting for transfers between devices, body(): weight_grad = lax.psum(owned, 'sp')  87 us
    reduce_scatter x1, waiting for transfers between devices, body(): lax.psum_scatter(weight_terms(key_grads, token_rows), 'dp', scatter_dimen...  85.4 us
    unnamed x4, other arithmetic  63.3 us
    unnamed x39, local copies, waits for them, and re-layouts  44.9 us
    all_to_all x1, blocking collectives, body(): lax.all_to_all(grad_key.reshape(1, seq_len, -1), 'sp', split_axis=1, conc...  22.8 us
    dot_general x9, matrix products, product(): return jnp.einsum(form, left, right, preferred_element_type=jnp.float32)  20.1 us
    all_gather x1, waiting for transfers between devices, body(): gathered = lax.all_gather(key_weight, 'dp', axis=0, tiled=True)  14.1 us
    concatenate x2, other arithmetic, unrotate(): jnp.concatenate([front * cosine + back * sine, back * cosine - front * si...  13.5 us
  transfers between devices with their start and end apart: 5, of which 3 were waited for; matrix products, arithmetic and copies ran while one was open for 25% of the time, Pallas kernels for 0%

commit v1 on v0

v1 whole, which is shorter than its diff:
```python
import functools

import jax
import jax.numpy as jnp
import numpy as np
from jax import lax
from jax.experimental import pallas as pl
from jax.experimental.pallas import tpu as pltpu
from jax.sharding import PartitionSpec as P

MESH = pl.DeviceIdType.MESH
F32, BF16 = jnp.float32, jnp.bfloat16
BLOCK = 128
NB = 32
WIDTH = 2048
C1 = 1280
CH = C1 // 2
C2 = WIDTH - C1
FACTOR = BLOCK**-0.5


def tables():
    half = 64
    freq = 10000.0 ** (-np.arange(half, dtype=np.float64) / half)
    freq = np.concatenate([freq, freq])
    sign = np.where(np.arange(128) < half, -1.0, 1.0)
    ang_j = np.arange(128, dtype=np.float64)[:, None] * freq
    ang_n = 128.0 * np.arange(NB, dtype=np.float64)[:, None] * freq
    inside = np.stack([np.cos(ang_j), np.sin(ang_j), sign * np.cos(ang_j), sign * np.sin(ang_j)])
    across = np.stack([np.cos(ang_n), np.sin(ang_n)], axis=1)
    return inside.astype(np.float32), across.astype(np.float32)


def dot(a, b, ca, cb):
    return lax.dot_general(a, b, (((ca,), (cb,)), ((), ())), preferred_element_type=F32)


SCRATCH = dict(
    tok=((512, WIDTH), BF16),
    wall=((8, 128, WIDTH), BF16),
    vv=((NB, 128, 256), BF16),
    rq=((NB, 128, 128), BF16),
    dq=((NB, 128, 128), BF16),
    cosv=((NB, 128, 128), F32),
    sinv=((NB, 128, 128), F32),
    jtv=((4, 128, 128), F32),
    ntv=((NB, 2, 128), F32),
    within=((128, 128), F32),
    rise=((128, 128), F32),
    fall=((128, 128), F32),
    cot=((NB, 128, 256), BF16),
    mix=((NB, 128, 128), BF16),
    trl=((NB, 128, 256), F32),
    trb=((NB, 128, 256), BF16),
    gko=((NB, 128, 128), BF16),
    gki=((4, 128, 1024), BF16),
    keyo=((8, 4, 128, 128), BF16),
    keyi=((NB, 128, 128), BF16),
    ent=((128, 256), F32),
    gts=((256, WIDTH), BF16),
    gtr=((256, WIDTH), BF16),
    gtb=((256, WIDTH), BF16),
    gqb=((NB, 128, 128), BF16),
    gvb=((NB, 128, 256), BF16),
    dwz=((8, 128, C1), BF16),
    rz=((2, 7, 128, CH), BF16),
    dwx=((16, 8, 8, C2), BF16),
    rx=((16, 8, 8, C2), BF16),
    zx=((8, 8, C2), BF16),
    zr=((8, 8, C2), BF16),
    px=((16, 8, C1), BF16),
    pr=((16, 8, C1), BF16),
    fin=((16, 8, WIDTH), BF16),
    dwo=((16, 8, WIDTH), F32),
)
SEMS = dict(
    loc=6, cot_s=16, cot_r=16, tok_s=1, tok_r=1, wp_s=4, wp_r=4, wm_s=4, wm_r=4, gk_s=16, gk_r=16, key_s=16, key_r=16,
    gt_s=1, gt_r=1, rz_s=14, rz_r=14, rx_s=16, rx_r=16, zx_s=8, zx_r=8, px_s=16, px_r=16, fin_s=16, fin_r=16, out=4,
)


def kernel(ld_ref, jt_ref, nt_ref, tok_ref, w_ref, q_ref, v_ref, cot_ref, gt_o, gq_o, gv_o, dw_o, *scratch):
    s = dict(zip([*SCRATCH, *SEMS], scratch, strict=True))
    B = type("B", (), s)
    sp, dp = lax.axis_index("sp"), lax.axis_index("dp")
    y, x = lax.div(sp, 4), lax.rem(sp, 4)
    z, c = lax.div(dp, 2), lax.rem(dp, 2)
    head_core = lax.rem(x, 2)
    head_at = lax.div(sp, 2)

    def plane(t):
        def off(u):
            return lax.rem(2 + u + lax.div(u, 2) + 2 * lax.div(u, 3), 4)

        dy, dx = off(lax.div(t, 4)), off(lax.rem(t, 4))
        to = lax.rem(y + dy, 4) * 4 + lax.rem(x + dx, 4)
        of = lax.rem(y + 4 - dy, 4) * 4 + lax.rem(x + 4 - dx, 4)
        return to, of

    def zdev(dz, core=c):
        return lax.rem(z + 8 + dz, 8) * 2 + core

    def remote(src, dst, ss, rs, dev):
        return pltpu.make_async_remote_copy(
            src_ref=src, dst_ref=dst, send_sem=ss, recv_sem=rs, device_id=dev, device_id_type=MESH
        )

    def arrived(ref, sem):
        pltpu.make_async_copy(ref, ref, sem).wait()

    def loop(lo, hi, f):
        def step(i, carry):
            f(i)
            return carry

        lax.fori_loop(lo, hi, step, 0)

    bar = pltpu.get_barrier_semaphore()
    partner = (sp, zdev(0, 1 - c))

    def greet(k):
        for core in (c, 1 - c):
            pl.semaphore_signal(bar, inc=1, device_id=(lax.rem(sp + k, 16), zdev(0, core)), device_id_type=MESH)

    def greet_z(k):
        pl.semaphore_signal(bar, inc=1, device_id=(sp, zdev(k)), device_id_type=MESH)

    loads = [
        pltpu.make_async_copy(q_ref, B.rq, B.loc.at[0]),
        pltpu.make_async_copy(v_ref, B.vv, B.loc.at[1]),
        pltpu.make_async_copy(tok_ref, B.tok.at[pl.ds(c * 256, 256)], B.loc.at[2]),
        pltpu.make_async_copy(w_ref, B.wall.at[z], B.loc.at[3]),
        pltpu.make_async_copy(jt_ref, B.jtv, B.loc.at[4]),
        pltpu.make_async_copy(nt_ref, B.ntv, B.loc.at[5]),
    ]
    for cp in loads:
        cp.start()
    own_cot = pltpu.make_async_copy(
        cot_ref.at[:, :, pl.ds(pl.multiple_of(sp * 256, 256), 256)], B.cot.at[pl.ds(2 * sp, 2)], B.cot_r.at[sp]
    )
    own_cot.start()

    loop(1, 16, greet)
    pl.semaphore_signal(bar, inc=1, device_id=partner, device_id_type=MESH)
    loop(1, 8, greet_z)
    pl.semaphore_wait(bar, 38)

    up, down = (sp, zdev(1)), (sp, zdev(-1))
    w_up = remote(w_ref, B.wall.at[z], B.wp_s.at[0], B.wp_r.at[0], up)
    w_down = remote(w_ref, B.wall.at[z], B.wm_s.at[0], B.wm_r.at[0], down)
    w_up.start()
    w_down.start()

    def cot_copy(t):
        to, _ = plane(t)
        return remote(
            cot_ref.at[:, :, pl.ds(pl.multiple_of(to * 256, 256), 256)],
            B.cot.at[pl.ds(2 * sp, 2)],
            B.cot_s.at[t],
            B.cot_r.at[sp],
            (to, dp),
        )

    loop(0, 15, lambda t: cot_copy(t).start())
    tok_copy = remote(tok_ref, B.tok.at[pl.ds(c * 256, 256)], B.tok_s.at[0], B.tok_r.at[0], partner)
    tok_copy.start()

    ld = ld_ref[sp]
    rows = lax.broadcasted_iota(jnp.int32, (128, 128), 0).astype(F32)
    cols = lax.broadcasted_iota(jnp.int32, (128, 128), 1).astype(F32)
    offset = rows - cols
    B.within[...] = jnp.where(offset >= 0, jnp.exp(jnp.maximum(offset, 0.0) * ld), 0.0)
    B.rise[...] = jnp.exp((rows + 1.0) * ld)
    B.fall[...] = jnp.exp((127.0 - rows) * ld)
    growth = jnp.exp(jnp.full((1, 256), 128.0, F32) * ld)
    loads[4].wait()
    loads[5].wait()
    loads[0].wait()

    def turn(n):
        cn, sn = B.ntv[n, 0:1, :], B.ntv[n, 1:2, :]
        cosine = cn * B.jtv[0] - sn * B.jtv[1]
        sine = sn * B.jtv[2] + cn * B.jtv[3]
        B.cosv[n] = cosine
        B.sinv[n] = sine
        u = B.rq[n].astype(F32)
        r = (u * cosine + pltpu.roll(u, 64, 1) * sine).astype(BF16)
        B.rq[n] = r
        B.dq[n] = (r.astype(F32) * B.rise[...]).astype(BF16)

    loop(0, NB, turn)

    def keys(hh):
        def part(i):
            k = dot(B.tok[pl.ds(pl.multiple_of(i * 256, 256), 256), :], B.wall[hh], 1, 1)
            B.keyo[hh, pl.ds(2 * i, 2)] = k.astype(BF16).reshape(2, 128, 128)

        loop(0, 2, part)

    def zat(dz):
        return lax.rem(z + 8 + dz, 8)

    loads[2].wait()
    arrived(B.tok.at[pl.ds((1 - c) * 256, 256)], B.tok_r.at[0])
    loads[3].wait()

    def w_forward(k, rows_up, rows_down):
        a, b = zat(-k), zat(k)
        arrived(B.wall.at[a], B.wp_r.at[k - 1])
        fu = remote(B.wall.at[a, rows_up], B.wall.at[a, rows_up], B.wp_s.at[k], B.wp_r.at[k], up)
        fu.start()
        arrived(B.wall.at[b], B.wm_r.at[k - 1])
        fd = remote(B.wall.at[b, rows_down], B.wall.at[b, rows_down], B.wm_s.at[k], B.wm_r.at[k], down)
        fd.start()
        return fu, fd

    full = pl.ds(0, 128)

    def cot_chunk(t):
        _, p = plane(t)
        arrived(B.cot.at[pl.ds(2 * p, 2)], B.cot_r.at[p])
        for b in range(2):
            n = 2 * p + b
            cb = B.cot[n]
            m = dot(cb, B.vv[n], 1, 1) * B.within[...]
            B.mix[n] = m.astype(BF16)
            B.trl[n] = dot(B.dq[n], cb, 0, 0)

    loads[1].wait()
    f1 = w_forward(1, full, full)
    loop(0, 3, lambda i: keys(zat(i - 1)))
    loop(0, 8, cot_chunk)
    f2 = w_forward(2, full, full)
    loop(0, 2, lambda i: keys(zat(4 * i - 2)))
    loop(8, 16, cot_chunk)

    def scan(i, carry):
        n = NB - 1 - i
        B.trb[n] = carry.astype(BF16)
        return B.trl[n] + growth * carry

    lax.fori_loop(0, NB, scan, jnp.zeros((128, 256), F32))

    def gk_copy(t):
        to, _ = plane(t)
        return remote(
            B.gko.at[pl.ds(2 * to, 2)],
            B.gki.at[pl.ds(2 * c, 2), :, pl.ds(pl.multiple_of(head_at * 128, 128), 128)],
            B.gk_s.at[t],
            B.gk_r.at[head_at * 2 + c],
            (to, zdev(0, head_core)),
        )

    def gk_chunk(t):
        p, _ = plane(t)
        for b in range(2):
            n = 2 * p + b
            g = dot(B.mix[n], B.rq[n], 0, 0) + B.fall[...] * dot(B.vv[n], B.trb[n], 1, 1)
            g = g * B.cosv[n] - pltpu.roll(g, 64, 1) * B.sinv[n]
            B.gko[n] = (g * FACTOR).astype(BF16)

    def gk_step(t):
        gk_chunk(t)
        gk_copy(t).start()

    loop(0, 15, gk_step)
    gk_chunk(15)

    @pl.when(head_core == c)
    def _():
        pltpu.make_async_copy(
            B.gko.at[pl.ds(2 * sp, 2)],
            B.gki.at[pl.ds(2 * c, 2), :, pl.ds(pl.multiple_of(head_at * 128, 128), 128)],
            B.gk_r.at[head_at * 2 + c],
        ).start()

    @pl.when(head_core != c)
    def _():
        gk_copy(15).start()

    f3 = w_forward(3, pl.ds(0, 64), pl.ds(64, 64))
    loop(0, 2, lambda i: keys(zat(6 * i - 3)))

    def key_copy(hh, i):
        return remote(
            B.keyo.at[hh, pl.ds(2 * i, 2)],
            B.keyi.at[pl.ds(2 * sp, 2)],
            B.key_s.at[2 * hh + i],
            B.key_r.at[sp],
            (2 * hh + c, zdev(0, i)),
        )

    def key_send(hh):
        for i in range(2):
            mine = jnp.logical_and(2 * hh + c == sp, c == i)

            @pl.when(mine)
            def _():
                pltpu.make_async_copy(
                    B.keyo.at[hh, pl.ds(2 * i, 2)], B.keyi.at[pl.ds(2 * sp, 2)], B.key_r.at[sp]
                ).start()

            @pl.when(jnp.logical_not(mine))
            def _():
                key_copy(hh, i).start()

    loop(0, 7, lambda i: key_send(zat(i - 3)))

    def gki_arrived(i):
        hh, j = lax.div(i, 2), lax.rem(i, 2)
        arrived(B.gki.at[pl.ds(2 * j, 2), :, pl.ds(pl.multiple_of(hh * 128, 128), 128)], B.gk_r.at[i])

    loop(0, 16, gki_arrived)

    def ring_copy(way, half, k):
        slot = (4 - k) if (way == half) else 4 + (3 - k)
        d = zat(k if way == 0 else -k)
        sem = way * 7 + slot
        return remote(
            B.dwz.at[d, :, pl.ds(half * CH, CH)],
            B.rz.at[way, slot],
            B.rz_s.at[sem],
            B.rz_r.at[sem],
            up if way == 0 else down,
        )

    def dw_head(t):
        r, i = lax.rem(t, 2), lax.div(t, 2)
        hh = zat(r * (3 - i) + (1 - r) * (4 + i))
        a = B.gki[:, :, pl.ds(pl.multiple_of(hh * 128, 128), 128)].reshape(512, 128)
        for lo in range(0, WIDTH, 256):
            g = dot(a, B.tok[:, lo : lo + 256], 0, 0)
            if lo < C1:
                B.dwz[hh, :, lo : lo + 256] = g.astype(BF16)
            else:
                B.dwx[:, hh, :, lo - C1 : lo - C1 + 256] = g.reshape(16, 8, 256).astype(BF16)

        @pl.when(t == 0)
        def _():
            ring_copy(0, 0, 4).start()
            ring_copy(1, 1, 4).start()

        @pl.when(t == 1)
        def _():
            ring_copy(0, 1, 3).start()

        @pl.when(t == 2)
        def _():
            ring_copy(1, 0, 3).start()

    loop(0, 8, dw_head)

    def rx_copy(t):
        to, _ = plane(t)
        return remote(B.dwx.at[to], B.rx.at[sp], B.rx_s.at[t], B.rx_r.at[sp], (to, dp))

    loop(0, 15, lambda t: rx_copy(t).start())

    arrived(B.wall.at[zat(4), pl.ds(0, 64)], B.wp_r.at[3])
    arrived(B.wall.at[zat(4), pl.ds(64, 64)], B.wm_r.at[3])
    loop(0, 1, lambda i: keys(zat(4)))
    key_send(zat(4))

    def gt_tile(first):
        def tile(i):
            lo = pl.multiple_of(i * 256, 256)
            j = (1 - c) if first else c
            a = jnp.concatenate([B.gki[2 * j], B.gki[2 * j + 1]], axis=0)
            w = B.wall[:, :, pl.ds(lo, 256)].reshape(1024, 256)
            g = dot(a, w, 1, 0)
            if first:
                B.gts[:, pl.ds(lo, 256)] = g.astype(BF16)
            else:
                B.gtb[:, pl.ds(lo, 256)] = (g + B.gtr[:, pl.ds(lo, 256)].astype(F32)).astype(BF16)

        return tile

    loop(0, 8, gt_tile(True))
    gt_copy = remote(B.gts, B.gtr, B.gt_s.at[0], B.gt_r.at[0], partner)
    gt_copy.start()

    def ring_take(way, half, k):
        slot = (4 - k) if (way == half) else 4 + (3 - k)
        arrived(B.rz.at[way, slot], B.rz_r.at[way * 7 + slot])
        if k == 1:
            return
        d = zat(k - 1 if way == 0 else 1 - k)

        def add(i):
            at = pl.ds(pl.multiple_of(i * 16, 16), 16)
            have = B.dwz[d, at, half * CH : half * CH + CH].astype(F32)
            B.dwz[d, at, half * CH : half * CH + CH] = (have + B.rz[way, slot, at, :].astype(F32)).astype(BF16)

        loop(0, 8, add)
        ring_copy(way, half, k - 1).start()

    ring_take(0, 0, 4)
    ring_take(1, 1, 4)
    arrived(B.gtr, B.gt_r.at[0])
    loop(0, 8, gt_tile(False))
    gt_out = pltpu.make_async_copy(B.gtb, gt_o, B.out.at[0])
    gt_out.start()
    for k in (3,):
        for way in (0, 1):
            for half in (way, 1 - way):
                ring_take(way, half, k)

    def keyi_arrived(p):
        arrived(B.keyi.at[pl.ds(2 * p, 2)], B.key_r.at[p])

    def back(n):
        u = B.keyi[n].astype(F32)
        rk = ((u * B.cosv[n] + pltpu.roll(u, 64, 1) * B.sinv[n]) * FACTOR).astype(BF16)
        cb = B.cot[n]
        sc = (dot(B.rq[n], rk, 1, 1) * B.within[...]).astype(BF16)
        e = B.ent[...]
        g = dot(B.mix[n], rk, 1, 0) + B.rise[...] * dot(cb, e.astype(BF16), 1, 1)
        B.gqb[n] = (g * B.cosv[n] - pltpu.roll(g, 64, 1) * B.sinv[n]).astype(BF16)
        f = B.fall[...]
        gv = dot(sc, cb, 0, 0)
        gt = dot(rk, B.trb[n], 1, 0)
        B.gvb[n, :, 0:128] = (gv[:, 0:128] + f * gt[:, 0:128]).astype(BF16)
        B.gvb[n, :, 128:256] = (gv[:, 128:256] + f * gt[:, 128:256]).astype(BF16)
        dk = (rk.astype(F32) * f).astype(BF16)
        B.ent[...] = dot(dk, B.vv[n], 0, 0) + growth * e

    B.ent[...] = jnp.zeros((128, 256), F32)
    loop(0, 16, keyi_arrived)
    loop(0, 16, back)

    for k in (2,):
        for way in (0, 1):
            for half in (way, 1 - way):
                ring_take(way, half, k)

    def rx_arrived(t):
        _, p = plane(t)
        arrived(B.rx.at[p], B.rx_r.at[p])

    loop(0, 15, rx_arrived)

    def plane_sum(d):
        total = B.dwx[sp, d].astype(F32)

        def more(t, acc):
            _, p = plane(t)
            return acc + B.rx[p, d].astype(F32)

        B.zx[d] = lax.fori_loop(0, 15, more, total).astype(BF16)

    loop(0, 8, plane_sum)

    def zx_copy(k):
        d = zat(k)
        return remote(B.zx.at[d], B.zr.at[z], B.zx_s.at[k], B.zx_r.at[z], (sp, zdev(k)))

    loop(1, 8, lambda k: zx_copy(k).start())

    loop(16, 32, back)
    gq_out = pltpu.make_async_copy(B.gqb, gq_o, B.out.at[1])
    gq_out.start()
    gv_out = pltpu.make_async_copy(B.gvb, gv_o, B.out.at[2])
    gv_out.start()

    for way in (0, 1):
        for half in (way, 1 - way):
            ring_take(way, half, 1)

    def owned(i):
        at = pl.ds(pl.multiple_of(i * 16, 16), 16)
        for half in range(2):
            v = B.dwz[z, at, half * CH : half * CH + CH].astype(F32)
            for way in range(2):
                slot = 3 if way == half else 6
                v += B.rz[way, slot, at, :].astype(F32)
            B.px[pl.ds(2 * i, 2), :, half * CH : half * CH + CH] = v.reshape(2, 8, CH).astype(BF16)

    loop(0, 8, owned)

    def px_copy(t):
        to, _ = plane(t)
        return remote(B.px.at[to], B.pr.at[sp], B.px_s.at[t], B.px_r.at[sp], (to, dp))

    loop(0, 15, lambda t: px_copy(t).start())

    def zr_arrived(k):
        d = zat(k)
        arrived(B.zr.at[d], B.zx_r.at[d])

    loop(1, 8, zr_arrived)
    total = lax.fori_loop(1, 8, lambda k, acc: acc + B.zr[zat(k)].astype(F32), B.zx[z].astype(F32))
    B.fin[sp, :, C1:WIDTH] = total.astype(BF16)

    def pr_arrived(t):
        _, p = plane(t)
        arrived(B.pr.at[p], B.px_r.at[p])

    loop(0, 15, pr_arrived)

    def pr_sum(t, acc):
        _, p = plane(t)
        return acc + B.pr[p].astype(F32)

    B.fin[sp, :, 0:C1] = lax.fori_loop(0, 15, pr_sum, B.px[sp].astype(F32)).astype(BF16)

    def fin_copy(t):
        to, _ = plane(t)
        return remote(B.fin.at[sp], B.fin.at[sp], B.fin_s.at[t], B.fin_r.at[sp], (to, dp))

    loop(0, 15, lambda t: fin_copy(t).start())

    def fin_arrived(t):
        _, p = plane(t)
        arrived(B.fin.at[p], B.fin_r.at[p])

    loop(0, 15, fin_arrived)

    def widen(j):
        B.dwo[j] = B.fin[j].astype(F32)

    loop(0, 16, widen)
    dw_out = pltpu.make_async_copy(B.dwo, dw_o, B.out.at[3])
    dw_out.start()

    for cp in (w_up, w_down, *f1, *f2, *f3, tok_copy, gt_copy):
        cp.wait_send()
    for way in (0, 1):
        for k in (4, 3, 2, 1):
            for half in (0, 1):
                if k < 4 or way == half:
                    ring_copy(way, half, k).wait_send()

    def sent(t):
        cot_copy(t).wait_send()
        gk_copy(t).wait_send()
        rx_copy(t).wait_send()
        px_copy(t).wait_send()
        fin_copy(t).wait_send()

    loop(0, 15, sent)

    @pl.when(head_core != c)
    def _():
        gk_copy(15).wait_send()

    def key_sent(hh):
        for i in range(2):

            @pl.when(jnp.logical_not(jnp.logical_and(2 * hh + c == sp, c == i)))
            def _():
                key_copy(hh, i).wait_send()

    loop(0, 8, key_sent)
    loop(1, 8, lambda k: zx_copy(k).wait_send())
    for cp in (gt_out, gq_out, gv_out, dw_out):
        cp.wait()


def body(tokens, key_weight, queries, values, cotangent, log_decay):
    inside, across = tables()
    any_space = pl.BlockSpec(memory_space=pl.ANY)
    shapes = [
        jax.ShapeDtypeStruct((256, WIDTH), BF16),
        jax.ShapeDtypeStruct((NB, 128, 128), BF16),
        jax.ShapeDtypeStruct((NB, 128, 256), BF16),
        jax.ShapeDtypeStruct((16, 8, WIDTH), F32),
    ]
    gt, gq, gv, dw = pl.pallas_call(
        kernel,
        out_shape=shapes,
        in_specs=[pl.BlockSpec(memory_space=pltpu.SMEM)] + [any_space] * 7,
        out_specs=[any_space] * 4,
        scratch_shapes=[pltpu.VMEM(shape, kind) for shape, kind in SCRATCH.values()]
        + [pltpu.SemaphoreType.DMA((n,)) for n in SEMS.values()],
        compiler_params=pltpu.CompilerParams(
            collective_id=0, has_side_effects=True, vmem_limit_bytes=58 * 2**20
        ),
        name="retention",
    )(
        log_decay,
        inside,
        across,
        tokens.reshape(256, WIDTH),
        key_weight,
        queries.reshape(NB, 128, 128),
        values.reshape(NB, 128, 256),
        cotangent.reshape(2, 128, 4096),
    )
    return (
        gt.reshape(1, 256, WIDTH),
        gq.reshape(1, 4096, 1, 128),
        gv.reshape(1, 4096, 1, 256),
        dw.reshape(128, WIDTH),
    )


def solution(mesh):
    return jax.shard_map(
        body,
        mesh=mesh,
        in_specs=(
            P("dp", "sp", None),
            P("dp", None),
            P("dp", None, "sp", None),
            P("dp", None, "sp", None),
            P("dp", "sp", None),
            P(),
        ),
        out_specs=(
            P("dp", "sp", None),
            P("dp", None, "sp", None),
            P("dp", None, "sp", None),
            P("dp", None),
        ),
        check_vma=False,
    )
```

time: 457 us -> 140 us (0.31); the launches traced: 448 us -> 140 us
  waiting for transfers between devices: 187 us -> 0 us
  Pallas kernels: 0 us -> 133 us
  other arithmetic: 92 us -> 0 us
  local copies, waits for them, and re-layouts: 63 us -> 6.36 us
  matrix products: 53.4 us -> 0 us
  blocking collectives: 22.8 us -> 0 us
  starting transfers between devices: 15.2 us -> 0 us
  between operations: 14.9 us -> 0.66 us
    pallas_call x0 -> x1, Pallas kernels: none -> 133 us  [body(): pl.pallas_call(kernel, out_shape=shapes, in_specs=[pl.BlockSpec(memory_sp...]
    psum x1 -> x0, waiting for transfers between devices: 87 us -> none  [body(): weight_grad = lax.psum(owned, 'sp')]
    reduce_scatter x1 -> x0, waiting for transfers between devices: 85.4 us -> none  [body(): lax.psum_scatter(weight_terms(key_grads, token_rows), 'dp', scatter_dimen...]
    unnamed x4 -> x0, other arithmetic: 63.3 us -> none
    dot_general x14 -> x0, matrix products: 53.4 us -> none  [the longest x9 20.1 us: product(): return jnp.einsum(form, left, right, preferred_element_type=jnp.float32)]
    unnamed x39 -> x10, local copies, waits for them, and re-layouts: 44.9 us -> 6.36 us
    all_to_all x1 -> x0, blocking collectives: 22.8 us -> none  [body(): lax.all_to_all(grad_key.reshape(1, seq_len, -1), 'sp', split_axis=1, conc...]
    all_to_all x2 -> x0, starting transfers between devices: 14.3 us -> none  [the longest x1 7.73 us: body(): lax.all_to_all(cotangent, 'sp', split_axis=2, concat_axis=1, tiled=True)]
  transfers between devices with their start and end apart: 5 -> 0, of which waited for: 3 -> 0; matrix products, arithmetic and copies ran while one was open for 25% -> 0% of each run, Pallas kernels for 0% -> 0%
where the time goes in v1:
time: 140 us
  Pallas kernels  133 us (95%)
  local copies, waits for them, and re-layouts  6.36 us (5%)
    pallas_call x1, Pallas kernels, body(): pl.pallas_call(kernel, out_shape=shapes, in_specs=[pl.BlockSpec(memory_sp...  133 us
    unnamed x10, local copies, waits for them, and re-layouts  6.36 us

profile of v1, /device:TPU:1, one launch (start us, length us, event | category | flops | bytes accessed | tf_op | source)
XLA Modules:
  0.0 139.9 jit_solution(16975235910024775781)
XLA Ops:
  0.6 132.8 %retention.1 = (bf16[256,2048]{1,0:T(8,128)(2,1)}, bf16[32,128,128]{2,1,0:T(8,128)(2,1)}, bf16[32,128,256]{2,1,0:T(8,128)(2,1)}, f32[16,8,2048]{2,1,0:T(8,128)}) custom-call(f32[16]{0:T(128)} %ld_ref.1, f32[4,128,128]{2,1,0:T(8,128)} %constant.4.clone.jt_ref, f32[32,2,128]{2,1,0:T(2,128)} %constant.5.clone.nt_ref, bf16[256,2048]{1,0:T(8,128)(2,1)} %bitcast.11, ...), custom_call_target="tpu_custom_call" | custom-call | tf_op jit(solution)/shard_map/retention/pallas_call | solution.py:568
  133.5 0.0 copy-start.2
  133.5 0.0 copy-start
  133.5 2.5 %copy.16 = bf16[1,256,2048]{2,1,0:T(8,128)(2,1)} copy(bf16[1,256,2048]{2,1,0:T(8,128)(2,1)} %bitcast.15) | data formatting | bytes 2097152
  136.0 0.0 copy-done.2
  136.0 1.0 copy.17
  136.9 0.0 copy-done
  136.9 0.0 copy-start.1
  136.9 1.3 copy.18
  138.3 0.6 copy-done.1
  138.9 1.0 copy.19
Async XLA Ops:
  133.5 2.5 %copy-start.2 = (bf16[32,128,128]{2,1,0:T(8,128)(2,1)S(1)}, bf16[32,128,128]{2,1,0:T(8,128)(2,1)}, u32[]{:S(2)}) copy-start(bf16[32,128,128]{2,1,0:T(8,128)(2,1)} %get-tuple-element.9) | copy-start | bytes 3145732
  133.5 3.4 %copy-start = (bf16[32,128,256]{2,1,0:T(8,128)(2,1)S(1)}, bf16[32,128,256]{2,1,0:T(8,128)(2,1)}, u32[]{:S(2)}) copy-start(bf16[32,128,256]{2,1,0:T(8,128)(2,1)} %get-tuple-element.10) | copy-start | bytes 6291460
  136.9 2.0 %copy-start.1 = (f32[16,8,2048]{2,1,0:T(8,128)S(1)}, f32[16,8,2048]{2,1,0:T(8,128)}, u32[]{:S(2)}) copy-start(f32[16,8,2048]{2,1,0:T(8,128)} %get-tuple-element.11) | copy-start | bytes 3145732

commit v2 on v1

v2 whole, which is shorter than its diff:
```python
import functools

import jax
import jax.numpy as jnp
import numpy as np
from jax import lax
from jax.experimental import pallas as pl
from jax.experimental.pallas import tpu as pltpu
from jax.sharding import PartitionSpec as P

MESH = pl.DeviceIdType.MESH
F32, BF16 = jnp.float32, jnp.bfloat16
BLOCK = 128
NB = 32
WIDTH = 2048
WA, WB = 640, 640
C1 = WA + WB
C2 = WIDTH - C1
ORDER = sorted(
    ((dy, dx) for dy in range(4) for dx in range(4) if dy or dx),
    key=lambda d: (-min(d[0], 4 - d[0]) - min(d[1], 4 - d[1]), -min(d[0], 4 - d[0])),
) + [(0, 0)]
FACTOR = BLOCK**-0.5


def tables():
    half = 64
    freq = 10000.0 ** (-np.arange(half, dtype=np.float64) / half)
    freq = np.concatenate([freq, freq])
    sign = np.where(np.arange(128) < half, -1.0, 1.0)
    ang_j = np.arange(128, dtype=np.float64)[:, None] * freq
    ang_n = 128.0 * np.arange(NB, dtype=np.float64)[:, None] * freq
    inside = np.stack([np.cos(ang_j), np.sin(ang_j), sign * np.cos(ang_j), sign * np.sin(ang_j)])
    across = np.stack([np.cos(ang_n), np.sin(ang_n)], axis=1)
    return inside.astype(np.float32), across.astype(np.float32)


def dot(a, b, ca, cb):
    return lax.dot_general(a, b, (((ca,), (cb,)), ((), ())), preferred_element_type=F32)


SCRATCH = dict(
    tok=((512, WIDTH), BF16),
    wall=((8, 128, WIDTH), BF16),
    vv=((NB, 128, 256), BF16),
    rq=((NB, 128, 128), BF16),
    dq=((NB, 128, 128), BF16),
    cosv=((NB, 128, 128), F32),
    sinv=((NB, 128, 128), F32),
    jtv=((4, 128, 128), F32),
    ntv=((NB, 2, 128), F32),
    within=((128, 128), F32),
    rise=((128, 128), F32),
    fall=((128, 128), F32),
    cot=((NB, 128, 256), BF16),
    mix=((NB, 128, 128), BF16),
    trl=((NB, 128, 256), F32),
    trb=((NB, 128, 256), BF16),
    entb=((NB, 128, 256), BF16),
    gko=((NB, 128, 128), BF16),
    gki=((4, 128, 1024), BF16),
    keyo=((8, 4, 128, 128), BF16),
    keyi=((NB, 128, 128), BF16),
    gts=((256, WIDTH), BF16),
    gtr=((256, WIDTH), BF16),
    dwz=((8, 128, C1), BF16),
    rza=((2, 4, 128, WA), BF16),
    rzb=((2, 4, 128, WB), BF16),
    dwx=((16, 8, 8, C2), BF16),
    rx=((16, 8, 8, C2), BF16),
    zx=((8, 8, C2), BF16),
    zr=((8, 8, C2), BF16),
    px=((16, 8, C1), BF16),
    pr=((16, 8, C1), BF16),
    fin=((16, 8, WIDTH), BF16),
)
SEMS = dict(
    loc=6, cot_s=1, cot_r=16, tok_s=1, tok_r=1, w_s=1, wp_r=7, wm_r=7, gk_s=2, gk_r=1, key_s=2, key_r=1,
    gt_s=1, gt_r=1, rz_s=1, rz_r=16, rx_s=1, rx_r=1, zx_s=1, zx_r=1, px_s=1, px_r=1, fin_s=1, fin_r=1,
)


def kernel(ld_ref, jt_ref, nt_ref, tok_ref, w_ref, q_ref, v_ref, cot_ref, gt_o, gq_o, gv_o, dw_o, *scratch):
    B = type("B", (), dict(zip([*SCRATCH, *SEMS], scratch, strict=True)))
    sp, dp = lax.axis_index("sp"), lax.axis_index("dp")
    y, x = lax.div(sp, 4), lax.rem(sp, 4)
    z, c = lax.div(dp, 2), lax.rem(dp, 2)
    head_core = lax.rem(x, 2)
    head_at = lax.div(sp, 2)

    def plane(t):
        if isinstance(t, int):
            dy, dx = ORDER[t]
        else:
            code = jnp.int32(0)
            for k, (a, b) in enumerate(ORDER[:15]):
                code = jnp.where(t == k, a * 4 + b, code)
            dy, dx = lax.div(code, 4), lax.rem(code, 4)
        to = lax.rem(y + dy, 4) * 4 + lax.rem(x + dx, 4)
        of = lax.rem(y + 4 - dy, 4) * 4 + lax.rem(x + 4 - dx, 4)
        return to, of

    def zat(dz):
        return lax.rem(z + 8 + dz, 8)

    def zdev(dz, core=c):
        return zat(dz) * 2 + core

    def remote(src, dst, ss, rs, dev):
        return pltpu.make_async_remote_copy(
            src_ref=src, dst_ref=dst, send_sem=ss, recv_sem=rs, device_id=dev, device_id_type=MESH
        )

    def arrived(ref, sem):
        pltpu.make_async_copy(ref, ref, sem).wait()

    def loop(lo, hi, f):
        def step(i, carry):
            f(i)
            return carry

        lax.fori_loop(lo, hi, step, 0)

    def lanes(i, width=128):
        return pl.ds(pl.multiple_of(i * width, width), width)

    bar = pltpu.get_barrier_semaphore()
    partner = (sp, zdev(0, 1 - c))

    def greet(k):
        for core in (c, 1 - c):
            pl.semaphore_signal(bar, inc=1, device_id=(lax.rem(sp + k, 16), zdev(0, core)), device_id_type=MESH)

    loop(1, 16, greet)
    pl.semaphore_signal(bar, inc=1, device_id=partner, device_id_type=MESH)
    loop(1, 8, lambda k: pl.semaphore_signal(bar, inc=1, device_id=(sp, zdev(k)), device_id_type=MESH))

    loads = [
        pltpu.make_async_copy(q_ref, B.rq, B.loc.at[0]),
        pltpu.make_async_copy(v_ref, B.vv, B.loc.at[1]),
        pltpu.make_async_copy(tok_ref, B.tok.at[pl.ds(c * 256, 256)], B.loc.at[2]),
        pltpu.make_async_copy(w_ref, B.wall.at[z], B.loc.at[3]),
        pltpu.make_async_copy(jt_ref, B.jtv, B.loc.at[4]),
        pltpu.make_async_copy(nt_ref, B.ntv, B.loc.at[5]),
        pltpu.make_async_copy(cot_ref.at[:, :, lanes(sp, 256)], B.cot.at[pl.ds(2 * sp, 2)], B.cot_r.at[sp]),
    ]
    for cp in loads:
        cp.start()
    pl.semaphore_wait(bar, 38)

    up, down = (sp, zdev(1)), (sp, zdev(-1))

    def w_copy(k, part, way):
        at = zat(-k if way == 0 else k)
        rows = pl.ds(64 * part, 64)
        sem = (B.wp_r if way == 0 else B.wm_r).at[2 * k + part if k < 3 else 6]
        src = w_ref.at[rows] if k == 0 else B.wall.at[at, rows]
        return remote(src, B.wall.at[at, rows], B.w_s.at[0], sem, up if way == 0 else down)

    def w_step(k, part):
        for way in (0, 1):
            if k == 4:
                arrived(B.wall.at[zat(4), pl.ds(64 * way, 64)], (B.wp_r, B.wm_r)[way].at[6])
                continue
            at = zat(-k if way == 0 else k)
            arrived(B.wall.at[at, pl.ds(64 * part, 64)], (B.wp_r, B.wm_r)[way].at[2 * (k - 1) + part])
            if k < 3 or part == way:
                w_copy(k, part, way).start()

    for part in range(2):
        for way in (0, 1):
            w_copy(0, part, way).start()

    def cot_copy(t):
        to, _ = plane(t)
        return remote(
            cot_ref.at[:, :, lanes(to, 256)], B.cot.at[pl.ds(2 * sp, 2)], B.cot_s.at[0], B.cot_r.at[sp], (to, dp)
        )

    for t in range(15):
        cot_copy(t).start()
    tok_copy = remote(tok_ref, B.tok.at[pl.ds(c * 256, 256)], B.tok_s.at[0], B.tok_r.at[0], partner)
    tok_copy.start()

    ld = ld_ref[sp]
    rows = lax.broadcasted_iota(jnp.int32, (128, 128), 0).astype(F32)
    cols = lax.broadcasted_iota(jnp.int32, (128, 128), 1).astype(F32)
    offset = rows - cols
    B.within[...] = jnp.where(offset >= 0, jnp.exp(jnp.maximum(offset, 0.0) * ld), 0.0)
    B.rise[...] = jnp.exp((rows + 1.0) * ld)
    B.fall[...] = jnp.exp((127.0 - rows) * ld)
    growth = jnp.exp(jnp.full((1, 256), 128.0, F32) * ld)
    loads[4].wait()
    loads[5].wait()
    loads[0].wait()

    def turn(n):
        cn, sn = B.ntv[n, 0:1, :], B.ntv[n, 1:2, :]
        cosine = cn * B.jtv[0] - sn * B.jtv[1]
        sine = sn * B.jtv[2] + cn * B.jtv[3]
        B.cosv[n] = cosine
        B.sinv[n] = sine
        u = B.rq[n].astype(F32)
        r = (u * cosine + pltpu.roll(u, 64, 1) * sine).astype(BF16)
        B.rq[n] = r
        B.dq[n] = (r.astype(F32) * B.rise[...]).astype(BF16)

    loop(0, NB, turn)

    def keys(hh):
        def part(i):
            k = dot(B.tok[pl.ds(pl.multiple_of(i * 256, 256), 256), :], B.wall[hh], 1, 1)
            B.keyo[hh, pl.ds(2 * i, 2)] = k.astype(BF16).reshape(2, 128, 128)

        loop(0, 2, part)

    def key_copy(hh, i, sem):
        return remote(
            B.keyo.at[hh, pl.ds(2 * i, 2)],
            B.keyi.at[pl.ds(2 * sp, 2)],
            B.key_s.at[sem],
            B.key_r.at[0],
            (2 * hh + c, zdev(0, i)),
        )

    own_head_here = head_core == c

    def key_send(hh):
        for i in range(2):
            special = jnp.logical_and(hh == head_at, c == i)

            @pl.when(jnp.logical_and(special, own_head_here))
            def _():
                pltpu.make_async_copy(
                    B.keyo.at[hh, pl.ds(2 * i, 2)], B.keyi.at[pl.ds(2 * sp, 2)], B.key_r.at[0]
                ).start()

            @pl.when(jnp.logical_and(special, jnp.logical_not(own_head_here)))
            def _():
                key_copy(hh, i, 1).start()

            @pl.when(jnp.logical_not(special))
            def _():
                key_copy(hh, i, 0).start()

    def cot_chunk(t):
        _, p = plane(t)
        arrived(B.cot.at[pl.ds(2 * p, 2)], B.cot_r.at[p])
        for b in range(2):
            n = 2 * p + b
            cb = B.cot[n]
            m = dot(cb, B.vv[n], 1, 1) * B.within[...]
            B.mix[n] = m.astype(BF16)
            B.trl[n] = dot(B.dq[n], cb, 0, 0)

    loads[2].wait()
    arrived(B.tok.at[pl.ds((1 - c) * 256, 256)], B.tok_r.at[0])
    loads[3].wait()
    loads[1].wait()
    loop(0, 1, lambda i: keys(zat(0)))
    w_step(1, 0)
    loop(0, 3, cot_chunk)
    w_step(1, 1)
    loop(0, 2, lambda i: keys(zat(2 * i - 1)))
    loop(3, 7, cot_chunk)
    w_step(2, 0)
    loop(7, 12, cot_chunk)
    w_step(2, 1)
    loop(12, 16, cot_chunk)
    def scan(i, carry):
        n = NB - 1 - i
        B.trb[n] = carry.astype(BF16)
        return B.trl[n] + growth * carry

    lax.fori_loop(0, NB, scan, jnp.zeros((128, 256), F32))

    def gk_copy(t, sem=0):
        to, _ = plane(t)
        return remote(
            B.gko.at[pl.ds(2 * to, 2)],
            B.gki.at[pl.ds(2 * c, 2), :, lanes(head_at)],
            B.gk_s.at[sem],
            B.gk_r.at[0],
            (to, zdev(0, head_core)),
        )

    def gk_chunk(t):
        p, _ = plane(t)
        for b in range(2):
            n = 2 * p + b
            g = dot(B.mix[n], B.rq[n], 0, 0) + B.fall[...] * dot(B.vv[n], B.trb[n], 1, 1)
            g = g * B.cosv[n] - pltpu.roll(g, 64, 1) * B.sinv[n]
            B.gko[n] = (g * FACTOR).astype(BF16)

        @pl.when(t < 15)
        def _():
            gk_copy(t).start()

    loop(0, 8, gk_chunk)
    w_step(3, 0)
    loop(8, 16, gk_chunk)

    @pl.when(own_head_here)
    def _():
        pltpu.make_async_copy(
            B.gko.at[pl.ds(2 * sp, 2)], B.gki.at[pl.ds(2 * c, 2), :, lanes(head_at)], B.gk_r.at[0]
        ).start()

    @pl.when(jnp.logical_not(own_head_here))
    def _():
        gk_copy(15, 1).start()

    w_step(3, 1)
    loop(0, 4, lambda i: keys(zat(i - 3 + lax.div(i, 2) * 3)))

    arrived(B.gki, B.gk_r.at[0])
    def ring_refs(way, half, k):
        lo, width = (0, WA) if half == 0 else (WA, WB)
        return pl.ds(lo, width), (B.rza if half == 0 else B.rzb).at[way, k - 1], B.rz_r.at[(way * 2 + half) * 4 + k - 1]

    def ring_send(way, half, k):
        at, dst, sem = ring_refs(way, half, k)
        d = zat(k if way == 0 else -k)
        remote(B.dwz.at[d, :, at], dst, B.rz_s.at[0], sem, up if way == 0 else down).start()

    def ring_take(way, half, k):
        at, got, sem = ring_refs(way, half, k)
        arrived(got, sem)
        if k == 1:
            return
        d = zat(k - 1 if way == 0 else 1 - k)

        def add(i):
            r = pl.ds(pl.multiple_of(i * 16, 16), 16)
            B.dwz[d, r, at] = (B.dwz[d, r, at].astype(F32) + got[r, :].astype(F32)).astype(BF16)

        loop(0, 8, add)
        ring_send(way, half, k - 1)

    def dw_part(hh, lo, hi):
        a = B.gki[:, :, lanes(hh)].reshape(512, 128)
        for at in range(lo, hi, 256):
            g = dot(a, B.tok[:, at : at + 256], 0, 0)
            if at < C1:
                B.dwz[hh, :, at : at + 256] = g.astype(BF16)
            else:
                B.dwx[:, hh, :, at - C1 : at - C1 + 256] = g.reshape(16, 8, 256).astype(BF16)

    def dwz_head(t):
        r, i = lax.rem(t, 2), lax.div(t, 2)
        dw_part(zat(r * (3 - i) + (1 - r) * (4 + i)), 0, C1)

        @pl.when(t == 0)
        def _():
            ring_send(0, 0, 4)
            ring_send(1, 1, 4)

        @pl.when(t == 1)
        def _():
            ring_send(0, 1, 3)

        @pl.when(t == 2)
        def _():
            ring_send(1, 0, 3)

    loop(0, 3, dwz_head)
    loop(0, 8, lambda hh: dw_part(hh, C1, WIDTH))
    for t in range(15):
        to, _ = plane(t)
        remote(B.dwx.at[to], B.rx.at[sp], B.rx_s.at[0], B.rx_r.at[0], (to, dp)).start()
    def later(i):
        key_send(zat(lax.rem(sp + i, 7) - 3))

    loop(0, 7, later)
    loop(3, 8, dwz_head)
    ring_take(0, 0, 4)
    ring_take(1, 1, 4)
    w_step(4, 0)
    loop(0, 1, lambda i: keys(zat(4)))
    key_send(zat(4))
    ring_take(0, 1, 3)
    ring_take(1, 0, 3)

    def gt_tile(first):
        def tile(i):
            j = (1 - c) if first else c
            a = jnp.concatenate([B.gki[2 * j], B.gki[2 * j + 1]], axis=0)
            g = dot(a, B.wall[:, :, lanes(i, 256)].reshape(1024, 256), 1, 0)
            if first:
                B.gts[:, lanes(i, 256)] = g.astype(BF16)
            else:
                gt_o[:, lanes(i, 256)] = (g + B.gtr[:, lanes(i, 256)].astype(F32)).astype(BF16)

        return tile

    loop(0, 8, gt_tile(True))
    gt_copy = remote(B.gts, B.gtr, B.gt_s.at[0], B.gt_r.at[0], partner)
    gt_copy.start()
    ring_take(0, 0, 3)
    ring_take(1, 1, 3)
    arrived(B.gtr, B.gt_r.at[0])
    loop(0, 8, gt_tile(False))
    ring_take(0, 1, 2)
    ring_take(1, 0, 2)

    def back_a(i):
        for b in range(4):
            n = 4 * i + b
            u = B.keyi[n].astype(F32)
            rk = ((u * B.cosv[n] + pltpu.roll(u, 64, 1) * B.sinv[n]) * FACTOR).astype(BF16)
            B.keyi[n] = rk
            B.dq[n] = (dot(B.rq[n], rk, 1, 1) * B.within[...]).astype(BF16)
            dk = (rk.astype(F32) * B.fall[...]).astype(BF16)
            B.trl[n] = dot(dk, B.vv[n], 0, 0)

    def scan_up(n, carry):
        B.entb[n] = carry.astype(BF16)
        return B.trl[n] + growth * carry

    def back_c(i):
        for b in range(4):
            n = 4 * i + b
            rk, cb, f = B.keyi[n], B.cot[n], B.fall[...]
            g = dot(B.mix[n], rk, 1, 0) + B.rise[...] * dot(cb, B.entb[n], 1, 1)
            gq_o[n] = (g * B.cosv[n] - pltpu.roll(g, 64, 1) * B.sinv[n]).astype(BF16)
            near, far = dot(B.dq[n], cb, 0, 0), dot(rk, B.trb[n], 1, 0)
            for h in range(2):
                at = slice(128 * h, 128 * h + 128)
                gv_o[n, :, at] = (near[:, at] + f * far[:, at]).astype(BF16)

    ring_take(0, 0, 2)
    ring_take(1, 1, 2)
    ring_take(0, 1, 1)
    ring_take(1, 0, 1)
    arrived(B.rx.at[0:15], B.rx_r.at[0])
    B.rx[sp] = B.dwx[sp]

    def plane_sum(d):
        total = B.rx[0, d].astype(F32)
        for p in range(1, 16):
            total += B.rx[p, d].astype(F32)
        B.zx[d] = total.astype(BF16)

    loop(0, 8, plane_sum)
    for k in range(1, 8):
        d = zat(k)
        remote(B.zx.at[d], B.zr.at[z], B.zx_s.at[0], B.zx_r.at[0], (sp, zdev(k))).start()
    ring_take(0, 0, 1)
    ring_take(1, 1, 1)

    def owned(i):
        r = pl.ds(pl.multiple_of(i * 16, 16), 16)
        for got, lo, width in ((B.rza, 0, WA), (B.rzb, WA, WB)):
            v = B.dwz[z, r, lo : lo + width].astype(F32)
            v += got[0, 0, r, :].astype(F32) + got[1, 0, r, :].astype(F32)
            B.px[pl.ds(2 * i, 2), :, lo : lo + width] = v.reshape(2, 8, width).astype(BF16)

    loop(0, 8, owned)
    for t in range(15):
        to, _ = plane(t)
        remote(B.px.at[to], B.pr.at[sp], B.px_s.at[0], B.px_r.at[0], (to, dp)).start()

    arrived(B.keyi, B.key_r.at[0])
    loop(0, 8, back_a)
    lax.fori_loop(0, NB, scan_up, jnp.zeros((128, 256), F32))

    arrived(B.zr.at[0:7], B.zx_r.at[0])
    B.zr[z] = B.zx[z]
    total = B.zr[0].astype(F32)
    for k in range(1, 8):
        total += B.zr[k].astype(F32)
    B.fin[sp, :, C1:WIDTH] = total.astype(BF16)
    B.pr[sp] = B.px[sp]
    arrived(B.pr.at[0:15], B.px_r.at[0])
    total = B.pr[0].astype(F32)
    for p in range(1, 16):
        total += B.pr[p].astype(F32)
    B.fin[sp, :, 0:C1] = total.astype(BF16)
    for t in range(15):
        to, _ = plane(t)
        remote(B.fin.at[sp], B.fin.at[sp], B.fin_s.at[0], B.fin_r.at[0], (to, dp)).start()
    loop(0, 8, back_c)
    arrived(B.fin.at[0:15], B.fin_r.at[0])

    def widen(j):
        dw_o[j] = B.fin[j].astype(F32)

    loop(0, 16, widen)

    arrived(B.cot.at[0:30], B.cot_s.at[0])
    arrived(B.wall.at[0:7], B.w_s.at[0])
    tok_copy.wait_send()
    gt_copy.wait_send()
    arrived(B.gko.at[0:30], B.gk_s.at[0])
    arrived(B.keyi.at[0:30], B.key_s.at[0])

    @pl.when(jnp.logical_not(own_head_here))
    def _():
        arrived(B.gko.at[0:2], B.gk_s.at[1])
        arrived(B.keyi.at[0:2], B.key_s.at[1])

    arrived(B.dwz.at[0:7], B.rz_s.at[0])
    arrived(B.dwx.at[0:15], B.rx_s.at[0])
    arrived(B.px.at[0:15], B.px_s.at[0])
    arrived(B.zx.at[0:7], B.zx_s.at[0])
    arrived(B.fin.at[0:15], B.fin_s.at[0])


def body(tokens, key_weight, queries, values, cotangent, log_decay):
    inside, across = tables()
    hbm, vmem = pl.BlockSpec(memory_space=pltpu.HBM), pl.BlockSpec(memory_space=pltpu.VMEM)
    shapes = [
        jax.ShapeDtypeStruct((256, WIDTH), BF16),
        jax.ShapeDtypeStruct((NB, 128, 128), BF16),
        jax.ShapeDtypeStruct((NB, 128, 256), BF16),
        jax.ShapeDtypeStruct((16, 8, WIDTH), F32),
    ]
    gt, gq, gv, dw = pl.pallas_call(
        kernel,
        out_shape=shapes,
        in_specs=[pl.BlockSpec(memory_space=pltpu.SMEM)] + [hbm] * 7,
        out_specs=[vmem] * 4,
        scratch_shapes=[pltpu.VMEM(shape, kind) for shape, kind in SCRATCH.values()]
        + [pltpu.SemaphoreType.DMA((n,)) for n in SEMS.values()],
        compiler_params=pltpu.CompilerParams(
            collective_id=0, has_side_effects=True, vmem_limit_bytes=48 * 2**20
        ),
        name="retention",
    )(
        log_decay,
        *(
            pltpu.with_memory_space_constraint(a, pltpu.HBM)
            for a in (
                jnp.asarray(inside),
                jnp.asarray(across),
                tokens.reshape(256, WIDTH),
                key_weight,
                queries.reshape(NB, 128, 128),
                values.reshape(NB, 128, 256),
                cotangent.reshape(2, 128, 4096),
            )
        ),
    )
    return (
        gt.reshape(1, 256, WIDTH),
        gq.reshape(1, 4096, 1, 128),
        gv.reshape(1, 4096, 1, 256),
        dw.reshape(128, WIDTH),
    )


def solution(mesh):
    return jax.shard_map(
        body,
        mesh=mesh,
        in_specs=(
            P("dp", "sp", None),
            P("dp", None),
            P("dp", None, "sp", None),
            P("dp", None, "sp", None),
            P("dp", "sp", None),
            P(),
        ),
        out_specs=(
            P("dp", "sp", None),
            P("dp", None, "sp", None),
            P("dp", None, "sp", None),
            P("dp", None),
        ),
        check_vma=False,
    )
```

time: 140 us -> 111 us (0.79)
  Pallas kernels: 133 us -> 106 us
  local copies, waits for them, and re-layouts: 6.36 us -> 4.88 us
    pallas_call x1, Pallas kernels: 133 us -> 106 us  [body(): pl.pallas_call(kernel, out_shape=shapes, in_specs=[pl.BlockSpec(memory_sp...]
    unnamed x10 -> x6, local copies, waits for them, and re-layouts: 6.36 us -> 4.88 us
where the time goes in v2:
time: 111 us
  Pallas kernels  106 us (95%)
  local copies, waits for them, and re-layouts  4.88 us (4%)
    pallas_call x1, Pallas kernels, body(): pl.pallas_call(kernel, out_shape=shapes, in_specs=[pl.BlockSpec(memory_sp...  106 us
    unnamed x6, local copies, waits for them, and re-layouts  4.88 us

profile of v2, /device:TPU:1, one launch (start us, length us, event | category | flops | bytes accessed | tf_op | source)
XLA Modules:
  0.0 111.2 jit_solution(5646716912798239943)
XLA Ops:
  0.6 0.0 copy-start
  0.6 0.6 copy-done
  1.3 105.7 %retention.1 = (bf16[256,2048]{1,0:T(8,128)(2,1)S(1)}, bf16[32,128,128]{2,1,0:T(8,128)(2,1)S(1)}, bf16[32,128,256]{2,1,0:T(8,128)(2,1)S(1)}, f32[16,8,2048]{2,1,0:T(8,128)S(1)}) custom-call(f32[16]{0:T(128)S(1)} %copy-done, f32[4,128,128]{2,1,0:T(8,128)} %constant.4.clone.jt_ref, f32[32,2,128]{2,1,0:T(2,128)} %constant.5.clone.nt_ref, ...), custom_call_target="tpu_custom_call" | custom-call | tf_op jit(solution)/shard_map/retention/pallas_call | solution.py:518
  107.0 1.0 copy.16
  107.9 1.0 copy.17
  108.9 1.3 %copy.18 = bf16[1,4096,1,256]{3,1,2,0:T(8,128)(2,1)} copy(bf16[1,4096,1,256]{3,1,2,0:T(8,128)(2,1)S(1)} %bitcast.8) | data formatting | bytes 4194304
  110.2 1.0 copy.19
Async XLA Ops:
  0.6 0.7 copy-start

commit v3 on v2

--- a/solution.py
+++ b/solution.py
@@ -13,13 +13,14 @@
 BLOCK = 128
 NB = 32
 WIDTH = 2048
-WA, WB = 640, 640
-C1 = WA + WB
+CHAINS, CW = 3, 256
+C1 = CHAINS * CW
 C2 = WIDTH - C1
-ORDER = sorted(
-    ((dy, dx) for dy in range(4) for dx in range(4) if dy or dx),
-    key=lambda d: (-min(d[0], 4 - d[0]) - min(d[1], 4 - d[1]), -min(d[0], 4 - d[0])),
-) + [(0, 0)]
+H2 = C2 // 2
+ORDER = (
+    (1, 1), (3, 3), (3, 1), (1, 3), (2, 1), (2, 3), (1, 2), (3, 2), (2, 2), (1, 0), (3, 0), (0, 2), (2, 0), (0, 1), (0, 3),
+    (0, 0),
+)
 FACTOR = BLOCK**-0.5
 
 
@@ -38,6 +39,13 @@
 def dot(a, b, ca, cb):
     return lax.dot_general(a, b, (((ca,), (cb,)), ((), ())), preferred_element_type=F32)
 
+
+QUARTERS = (
+    (((2, 0), (2, 1)), ((0, 2), (0, 3))),
+    (((1, 2), (1, 3)), ((3, 0), (3, 1))),
+    (((1, 0), (1, 1)), ((3, 2), (3, 3))),
+    (((0, 0), (0, 1)), ((2, 2), (2, 3))),
+)
 
 SCRATCH = dict(
     tok=((512, WIDTH), BF16),
@@ -59,15 +67,18 @@
     entb=((NB, 128, 256), BF16),
     gko=((NB, 128, 128), BF16),
     gki=((4, 128, 1024), BF16),
+    gkt=((1024, 512), BF16),
     keyo=((8, 4, 128, 128), BF16),
     keyi=((NB, 128, 128), BF16),
     gts=((256, WIDTH), BF16),
     gtr=((256, WIDTH), BF16),
     dwz=((8, 128, C1), BF16),
-    rza=((2, 4, 128, WA), BF16),
-    rzb=((2, 4, 128, WB), BF16),
-    dwx=((16, 8, 8, C2), BF16),
-    rx=((16, 8, 8, C2), BF16),
+    rz=((CHAINS, 2, 4, 128, CW), BF16),
+    dwx=((2, 4, 4, 8, 8, H2), BF16),
+    f1=((2, 2, 2, 8, 8, H2), BF16),
+    r1=((2, 2, 4, 8, 8, H2), BF16),
+    s1=((2, 4, 8, 8, H2), BF16),
+    r2=((2, 4, 8, 8, H2), BF16),
     zx=((8, 8, C2), BF16),
     zr=((8, 8, C2), BF16),
     px=((16, 8, C1), BF16),
@@ -75,13 +86,13 @@
     fin=((16, 8, WIDTH), BF16),
 )
 SEMS = dict(
-    loc=6, cot_s=1, cot_r=16, tok_s=1, tok_r=1, w_s=1, wp_r=7, wm_r=7, gk_s=2, gk_r=1, key_s=2, key_r=1,
-    gt_s=1, gt_r=1, rz_s=1, rz_r=16, rx_s=1, rx_r=1, zx_s=1, zx_r=1, px_s=1, px_r=1, fin_s=1, fin_r=1,
+    loc=7, cot_s=1, cot_r=16, tok_s=1, tok_r=1, w_s=1, wp_r=7, wm_r=7, gk_s=2, gk_r=1, key_s=2, key_r=1,
+    gt_s=1, gt_r=1, rz_s=1, rz_r=8 * CHAINS, f1_r=4, r1_s=1, r1_r=1, r2_s=1, r2_r=1, zx_s=1, zx_r=1, px_s=1, px_r=1, fin_s=1, finx_r=1, finz_r=1,
 )
 
 
 def kernel(ld_ref, jt_ref, nt_ref, tok_ref, w_ref, q_ref, v_ref, cot_ref, gt_o, gq_o, gv_o, dw_o, *scratch):
-    B = type("B", (), dict(zip([*SCRATCH, *SEMS], scratch, strict=True)))
+    B = type("B", (), dict(zip([*SCRATCH, *SEMS, "lds"], scratch, strict=True)))
     sp, dp = lax.axis_index("sp"), lax.axis_index("dp")
     y, x = lax.div(sp, 4), lax.rem(sp, 4)
     z, c = lax.div(dp, 2), lax.rem(dp, 2)
@@ -136,6 +147,7 @@
     loop(1, 8, lambda k: pl.semaphore_signal(bar, inc=1, device_id=(sp, zdev(k)), device_id_type=MESH))
 
     loads = [
+        pltpu.make_async_copy(ld_ref, B.lds, B.loc.at[6]),
         pltpu.make_async_copy(q_ref, B.rq, B.loc.at[0]),
         pltpu.make_async_copy(v_ref, B.vv, B.loc.at[1]),
         pltpu.make_async_copy(tok_ref, B.tok.at[pl.ds(c * 256, 256)], B.loc.at[2]),
@@ -182,7 +194,8 @@
     tok_copy = remote(tok_ref, B.tok.at[pl.ds(c * 256, 256)], B.tok_s.at[0], B.tok_r.at[0], partner)
     tok_copy.start()
 
-    ld = ld_ref[sp]
+    loads[0].wait()
+    ld = B.lds[sp]
     rows = lax.broadcasted_iota(jnp.int32, (128, 128), 0).astype(F32)
     cols = lax.broadcasted_iota(jnp.int32, (128, 128), 1).astype(F32)
     offset = rows - cols
@@ -190,9 +203,9 @@
     B.rise[...] = jnp.exp((rows + 1.0) * ld)
     B.fall[...] = jnp.exp((127.0 - rows) * ld)
     growth = jnp.exp(jnp.full((1, 256), 128.0, F32) * ld)
-    loads[4].wait()
     loads[5].wait()
-    loads[0].wait()
+    loads[6].wait()
+    loads[1].wait()
 
     def turn(n):
         cn, sn = B.ntv[n, 0:1, :], B.ntv[n, 1:2, :]
@@ -253,26 +266,25 @@
             B.mix[n] = m.astype(BF16)
             B.trl[n] = dot(B.dq[n], cb, 0, 0)
 
-    loads[2].wait()
-    arrived(B.tok.at[pl.ds((1 - c) * 256, 256)], B.tok_r.at[0])
-    loads[3].wait()
-    loads[1].wait()
-    loop(0, 1, lambda i: keys(zat(0)))
-    w_step(1, 0)
-    loop(0, 3, cot_chunk)
-    w_step(1, 1)
-    loop(0, 2, lambda i: keys(zat(2 * i - 1)))
-    loop(3, 7, cot_chunk)
-    w_step(2, 0)
-    loop(7, 12, cot_chunk)
-    w_step(2, 1)
-    loop(12, 16, cot_chunk)
+    def take_tokens():
+        loads[3].wait()
+        arrived(B.tok.at[pl.ds((1 - c) * 256, 256)], B.tok_r.at[0])
+        loads[4].wait()
+        loads[2].wait()
+
+    def keys_of(first, step, count):
+        loop(0, count, lambda i: keys(zat(first + step * i)))
+
+    def mixing(lo, hi):
+        loop(lo, hi, cot_chunk)
+
     def scan(i, carry):
         n = NB - 1 - i
         B.trb[n] = carry.astype(BF16)
         return B.trl[n] + growth * carry
 
-    lax.fori_loop(0, NB, scan, jnp.zeros((128, 256), F32))
+    def trails():
+        lax.fori_loop(0, NB, scan, jnp.zeros((128, 256), F32))
 
     def gk_copy(t, sem=0):
         to, _ = plane(t)
@@ -296,90 +308,190 @@
         def _():
             gk_copy(t).start()
 
-    loop(0, 8, gk_chunk)
-    w_step(3, 0)
-    loop(8, 16, gk_chunk)
-
-    @pl.when(own_head_here)
-    def _():
-        pltpu.make_async_copy(
-            B.gko.at[pl.ds(2 * sp, 2)], B.gki.at[pl.ds(2 * c, 2), :, lanes(head_at)], B.gk_r.at[0]
-        ).start()
-
-    @pl.when(jnp.logical_not(own_head_here))
-    def _():
-        gk_copy(15, 1).start()
-
-    w_step(3, 1)
-    loop(0, 4, lambda i: keys(zat(i - 3 + lax.div(i, 2) * 3)))
-
-    arrived(B.gki, B.gk_r.at[0])
-    def ring_refs(way, half, k):
-        lo, width = (0, WA) if half == 0 else (WA, WB)
-        return pl.ds(lo, width), (B.rza if half == 0 else B.rzb).at[way, k - 1], B.rz_r.at[(way * 2 + half) * 4 + k - 1]
-
-    def ring_send(way, half, k):
-        at, dst, sem = ring_refs(way, half, k)
+    def key_grads(lo, hi):
+        loop(lo, hi, gk_chunk)
+        if hi < 16:
+            return
+
+        @pl.when(own_head_here)
+        def _():
+            pltpu.make_async_copy(
+                B.gko.at[pl.ds(2 * sp, 2)], B.gki.at[pl.ds(2 * c, 2), :, lanes(head_at)], B.gk_r.at[0]
+            ).start()
+
+        @pl.when(jnp.logical_not(own_head_here))
+        def _():
+            gk_copy(15, 1).start()
+
+    def take_key_grads():
+        arrived(B.gki, B.gk_r.at[0])
+        for i in range(4):
+            B.gkt[:, 128 * i : 128 * i + 128] = B.gki[i].T
+
+    def send_keys(part):
+        even = lax.rem(x + c, 2) == 0
+        for (y0, x0), (y1, x1) in QUARTERS[part]:
+            to = lax.rem(y + jnp.where(even, y0, y1), 4) * 4 + lax.rem(x + jnp.where(even, x0, x1), 4)
+            key_send(lax.div(to, 2))
+
+    def ring_refs(chain, way, k):
+        at = pl.ds(chain * CW, CW)
+        return at, B.rz.at[chain, way, k - 1], B.rz_r.at[(chain * 2 + way) * 4 + k - 1]
+
+    def ring_send(chain, way, k):
+        at, dst, sem = ring_refs(chain, way, k)
         d = zat(k if way == 0 else -k)
         remote(B.dwz.at[d, :, at], dst, B.rz_s.at[0], sem, up if way == 0 else down).start()
 
-    def ring_take(way, half, k):
-        at, got, sem = ring_refs(way, half, k)
+    def ring_take(chain, way, k):
+        at, got, sem = ring_refs(chain, way, k)
         arrived(got, sem)
         if k == 1:
             return
         d = zat(k - 1 if way == 0 else 1 - k)
 
         def add(i):
-            r = pl.ds(pl.multiple_of(i * 16, 16), 16)
+            r = pl.ds(pl.multiple_of(i * 32, 32), 32)
             B.dwz[d, r, at] = (B.dwz[d, r, at].astype(F32) + got[r, :].astype(F32)).astype(BF16)
 
-        loop(0, 8, add)
-        ring_send(way, half, k - 1)
-
-    def dw_part(hh, lo, hi):
-        a = B.gki[:, :, lanes(hh)].reshape(512, 128)
-        for at in range(lo, hi, 256):
-            g = dot(a, B.tok[:, at : at + 256], 0, 0)
-            if at < C1:
-                B.dwz[hh, :, at : at + 256] = g.astype(BF16)
-            else:
-                B.dwx[:, hh, :, at - C1 : at - C1 + 256] = g.reshape(16, 8, 256).astype(BF16)
-
-    def dwz_head(t):
-        r, i = lax.rem(t, 2), lax.div(t, 2)
-        dw_part(zat(r * (3 - i) + (1 - r) * (4 + i)), 0, C1)
-
-        @pl.when(t == 0)
-        def _():
-            ring_send(0, 0, 4)
-            ring_send(1, 1, 4)
-
-        @pl.when(t == 1)
-        def _():
-            ring_send(0, 1, 3)
-
-        @pl.when(t == 2)
-        def _():
-            ring_send(1, 0, 3)
-
-    loop(0, 3, dwz_head)
-    loop(0, 8, lambda hh: dw_part(hh, C1, WIDTH))
-    for t in range(15):
-        to, _ = plane(t)
-        remote(B.dwx.at[to], B.rx.at[sp], B.rx_s.at[0], B.rx_r.at[0], (to, dp)).start()
-    def later(i):
-        key_send(zat(lax.rem(sp + i, 7) - 3))
-
-    loop(0, 7, later)
-    loop(3, 8, dwz_head)
-    ring_take(0, 0, 4)
-    ring_take(1, 1, 4)
-    w_step(4, 0)
-    loop(0, 1, lambda i: keys(zat(4)))
-    key_send(zat(4))
-    ring_take(0, 1, 3)
-    ring_take(1, 0, 3)
+        loop(0, 4, add)
+        ring_send(chain, way, k - 1)
+
+    def take(chain, k):
+        ring_take(chain, chain % 2, k)
+        if k > 1:
+            ring_take(chain, 1 - chain % 2, k - 1)
+
+    def weight_ring(lo, hi):
+        def tile(i):
+            g = dot(B.gkt[...], B.tok[:, lanes(i, CW)], 1, 0)
+            B.dwz[:, :, lanes(i, CW)] = g.astype(BF16).reshape(8, 128, CW)
+
+        loop(lo, hi, tile)
+        for chain in range(lo, hi):
+            ring_send(chain, chain % 2, 4)
+            ring_send(chain, 1 - chain % 2, 3)
+
+    def line(way, step):
+        if way == 0:
+            at = lax.rem(x + step, 4)
+            return at, x, (y * 4 + at, dp)
+        at = lax.rem(y + step, 4)
+        return at, y, (at * 4 + x, dp)
+
+    def weight_plane(way):
+        def tile(at, width):
+            g = dot(B.gkt[...], B.tok[:, pl.ds(C1 + way * H2 + at, width)], 1, 0)
+            g = g.astype(BF16).reshape(8, 4, 4, 8, width)
+            for yy in range(4):
+                for xx in range(4):
+                    a1, a2 = (xx, yy) if way == 0 else (yy, xx)
+                    B.dwx[way, a1, a2, :, :, pl.ds(at, width)] = g[:, yy, xx]
+
+        if H2 % 256 == 0:
+            loop(0, H2 // 256, lambda i: tile(pl.multiple_of(i * 256, 256), 256))
+        else:
+            for at in range(0, H2, 256):
+                tile(at, min(256, H2 - at))
+        for step in (1, 3):
+            near, _, dev = line(way, step)
+            far, _, _ = line(way, 2)
+            side = 0 if step == 1 else 1
+            through, own = pl.ds(2 * side, 2), pl.ds(2 - 2 * side, 2)
+            remote(B.dwx.at[way, far, through], B.f1.at[way, side], B.r1_s.at[0], B.f1_r.at[2 * way + side], dev).start()
+            remote(B.dwx.at[way, near, own], B.r1.at[way, side, own], B.r1_s.at[0], B.r1_r.at[0], dev).start()
+
+    def line_pass(way):
+        for step in (1, 3):
+            near, _, dev = line(way, step)
+            side = 0 if step == 1 else 1
+            arrived(B.f1.at[way, side], B.f1_r.at[2 * way + side])
+
+            def add(i):
+                j, hh = lax.div(i, 4), lax.rem(i, 4) * 2
+                have = B.dwx[way, near, 2 * side + j, pl.ds(hh, 2)].astype(F32)
+                B.dwx[way, near, 2 * side + j, pl.ds(hh, 2)] = (have + B.f1[way, side, j, pl.ds(hh, 2)].astype(F32)).astype(BF16)
+
+            loop(0, 8, add)
+            through = pl.ds(2 * side, 2)
+            remote(
+                B.dwx.at[way, near, through], B.r1.at[way, side, through], B.r1_s.at[0], B.r1_r.at[0], dev
+            ).start()
+
+    def line_sums():
+        arrived(B.r1, B.r1_r.at[0])
+        for way, me in ((0, x), (1, y)):
+
+            def add(i):
+                j, hh = lax.div(i, 4), lax.rem(i, 4) * 2
+                total = B.dwx[way, me, j, pl.ds(hh, 2)].astype(F32)
+                for side in range(2):
+                    total += B.r1[way, side, j, pl.ds(hh, 2)].astype(F32)
+                B.s1[way, j, pl.ds(hh, 2)] = total.astype(BF16)
+
+            loop(0, 16, add)
+        for step in (2, 1, 3):
+            for way in (0, 1):
+                at, me, dev = line(1 - way, step)
+                remote(B.s1.at[way, at], B.r2.at[way, me], B.r2_s.at[0], B.r2_r.at[0], dev).start()
+
+    def plane_sums():
+        arrived(B.r2.at[:, 0:3], B.r2_r.at[0])
+        for way, me in ((0, y), (1, x)):
+            B.r2[way, me] = B.s1[way, me]
+            for hh in range(8):
+                total = B.r2[way, 0, hh].astype(F32)
+                for p in range(1, 4):
+                    total += B.r2[way, p, hh].astype(F32)
+                B.zx[hh, :, way * H2 : way * H2 + H2] = total.astype(BF16)
+        for k in range(1, 8):
+            d = zat(k)
+            remote(B.zx.at[d], B.zr.at[z], B.zx_s.at[0], B.zx_r.at[0], (sp, zdev(k))).start()
+
+    def own_rows(i):
+        r = pl.ds(pl.multiple_of(i * 16, 16), 16)
+        for chain in range(CHAINS):
+            at = slice(chain * CW, chain * CW + CW)
+            v = B.dwz[z, r, at].astype(F32) + B.rz[chain, 0, 0, r, :].astype(F32) + B.rz[chain, 1, 0, r, :].astype(F32)
+            B.px[pl.ds(2 * i, 2), :, at] = v.reshape(2, 8, CW).astype(BF16)
+
+    def column_sums():
+        loop(0, 8, own_rows)
+        for t in range(15):
+            to, _ = plane(t)
+            remote(B.px.at[to], B.pr.at[sp], B.px_s.at[0], B.px_r.at[0], (to, dp)).start()
+
+    def total_of(ref, count):
+        total = ref[0].astype(F32)
+        for p in range(1, count):
+            total += ref[p].astype(F32)
+        return total.astype(BF16)
+
+    def fin_send(lo, hi, sem):
+        for t in range(15):
+            to, _ = plane(t)
+            ref = B.fin.at[sp, :, pl.ds(lo, hi - lo)]
+            remote(ref, ref, B.fin_s.at[0], sem, (to, dp)).start()
+
+    def finish_plane_part():
+        arrived(B.zr.at[0:7], B.zx_r.at[0])
+        B.zr[z] = B.zx[z]
+        B.fin[sp, :, C1:WIDTH] = total_of(B.zr, 8)
+        fin_send(C1, WIDTH, B.finx_r.at[0])
+
+    def finish_ring_part():
+        B.pr[sp] = B.px[sp]
+        arrived(B.pr.at[0:15], B.px_r.at[0])
+        B.fin[sp, :, 0:C1] = total_of(B.pr, 16)
+        fin_send(0, C1, B.finz_r.at[0])
+
+    def widen(j):
+        dw_o[j] = B.fin[j].astype(F32)
+
+    def weight_out():
+        arrived(B.fin.at[0:15, :, C1:WIDTH], B.finx_r.at[0])
+        arrived(B.fin.at[0:15, :, 0:C1], B.finz_r.at[0])
+        loop(0, 16, widen)
 
     def gt_tile(first):
         def tile(i):
@@ -393,15 +505,17 @@
 
         return tile
 
-    loop(0, 8, gt_tile(True))
     gt_copy = remote(B.gts, B.gtr, B.gt_s.at[0], B.gt_r.at[0], partner)
-    gt_copy.start()
-    ring_take(0, 0, 3)
-    ring_take(1, 1, 3)
-    arrived(B.gtr, B.gt_r.at[0])
-    loop(0, 8, gt_tile(False))
-    ring_take(0, 1, 2)
-    ring_take(1, 0, 2)
+
+    def token_grads_partner(lo, hi):
+        loop(lo, hi, gt_tile(True))
+        if hi == 8:
+            gt_copy.start()
+
+    def token_grads(lo, hi):
+        if lo == 0:
+            arrived(B.gtr, B.gt_r.at[0])
+        loop(lo, hi, gt_tile(False))
 
     def back_a(i):
         for b in range(4):
@@ -428,64 +542,80 @@
                 at = slice(128 * h, 128 * h + 128)
                 gv_o[n, :, at] = (near[:, at] + f * far[:, at]).astype(BF16)
 
-    ring_take(0, 0, 2)
-    ring_take(1, 1, 2)
-    ring_take(0, 1, 1)
-    ring_take(1, 0, 1)
-    arrived(B.rx.at[0:15], B.rx_r.at[0])
-    B.rx[sp] = B.dwx[sp]
-
-    def plane_sum(d):
-        total = B.rx[0, d].astype(F32)
-        for p in range(1, 16):
-            total += B.rx[p, d].astype(F32)
-        B.zx[d] = total.astype(BF16)
-
-    loop(0, 8, plane_sum)
-    for k in range(1, 8):
-        d = zat(k)
-        remote(B.zx.at[d], B.zr.at[z], B.zx_s.at[0], B.zx_r.at[0], (sp, zdev(k))).start()
-    ring_take(0, 0, 1)
-    ring_take(1, 1, 1)
-
-    def owned(i):
-        r = pl.ds(pl.multiple_of(i * 16, 16), 16)
-        for got, lo, width in ((B.rza, 0, WA), (B.rzb, WA, WB)):
-            v = B.dwz[z, r, lo : lo + width].astype(F32)
-            v += got[0, 0, r, :].astype(F32) + got[1, 0, r, :].astype(F32)
-            B.px[pl.ds(2 * i, 2), :, lo : lo + width] = v.reshape(2, 8, width).astype(BF16)
-
-    loop(0, 8, owned)
-    for t in range(15):
-        to, _ = plane(t)
-        remote(B.px.at[to], B.pr.at[sp], B.px_s.at[0], B.px_r.at[0], (to, dp)).start()
-
-    arrived(B.keyi, B.key_r.at[0])
-    loop(0, 8, back_a)
-    lax.fori_loop(0, NB, scan_up, jnp.zeros((128, 256), F32))
-
-    arrived(B.zr.at[0:7], B.zx_r.at[0])
-    B.zr[z] = B.zx[z]
-    total = B.zr[0].astype(F32)
-    for k in range(1, 8):
-        total += B.zr[k].astype(F32)
-    B.fin[sp, :, C1:WIDTH] = total.astype(BF16)
-    B.pr[sp] = B.px[sp]
-    arrived(B.pr.at[0:15], B.px_r.at[0])
-    total = B.pr[0].astype(F32)
-    for p in range(1, 16):
-        total += B.pr[p].astype(F32)
-    B.fin[sp, :, 0:C1] = total.astype(BF16)
-    for t in range(15):
-        to, _ = plane(t)
-        remote(B.fin.at[sp], B.fin.at[sp], B.fin_s.at[0], B.fin_r.at[0], (to, dp)).start()
-    loop(0, 8, back_c)
-    arrived(B.fin.at[0:15], B.fin_r.at[0])
-
-    def widen(j):
-        dw_o[j] = B.fin[j].astype(F32)
-
-    loop(0, 16, widen)
+    def take_keys():
+        arrived(B.keyi, B.key_r.at[0])
+
+    def scores(lo, hi):
+        loop(lo, hi, back_a)
+
+    def states():
+        lax.fori_loop(0, NB, scan_up, jnp.zeros((128, 256), F32))
+
+    def query_value_grads(lo, hi):
+        loop(lo, hi, back_c)
+
+    SCHEDULE = (
+        (take_tokens,),
+        (keys_of, 0, 1, 1),
+        (w_step, 1, 0),
+        (mixing, 0, 3),
+        (w_step, 1, 1),
+        (keys_of, -1, 2, 2),
+        (mixing, 3, 7),
+        (w_step, 2, 0),
+        (mixing, 7, 12),
+        (w_step, 2, 1),
+        (mixing, 12, 16),
+        (trails,),
+        (key_grads, 0, 8),
+        (w_step, 3, 0),
+        (key_grads, 8, 16),
+        (w_step, 3, 1),
+        (keys_of, -3, 1, 2),
+        (keys_of, 2, 1, 2),
+        (take_key_grads,),
+        (weight_plane, 0),
+        (weight_ring, 0, 2),
+        (weight_plane, 1),
+        (weight_ring, 2, 3),
+        (w_step, 4, 0),
+        (keys_of, 4, 1, 1),
+        (token_grads_partner, 0, 3),
+        (take, 0, 4),
+        (take, 1, 4),
+        (line_pass, 0),
+        (token_grads_partner, 3, 5),
+        (take, 2, 4),
+        (line_pass, 1),
+        (send_keys, 0),
+        (send_keys, 1),
+        (token_grads_partner, 5, 8),
+        (take, 0, 3),
+        (take, 1, 3),
+        (take, 2, 3),
+        (line_sums,),
+        (send_keys, 2),
+        (take, 0, 2),
+        (take, 1, 2),
+        (token_grads, 0, 4),
+        (take, 2, 2),
+        (token_grads, 4, 8),
+        (take, 0, 1),
+        (take, 1, 1),
+        (take, 2, 1),
+        (column_sums,),
+        (send_keys, 3),
+        (plane_sums,),
+        (finish_ring_part,),
+        (finish_plane_part,),
+        (take_keys,),
+        (scores, 0, 8),
+        (states,),
+        (query_value_grads, 0, 8),
+        (weight_out,),
+    )
+    for step in SCHEDULE:
+        step[0](*step[1:])
 
     arrived(B.cot.at[0:30], B.cot_s.at[0])
     arrived(B.wall.at[0:7], B.w_s.at[0])
@@ -500,10 +630,20 @@
         arrived(B.keyi.at[0:2], B.key_s.at[1])
 
     arrived(B.dwz.at[0:7], B.rz_s.at[0])
-    arrived(B.dwx.at[0:15], B.rx_s.at[0])
+    arrived(B.dwx.at[:, 0:3], B.r1_s.at[0])
+    arrived(B.s1.at[:, 0:3], B.r2_s.at[0])
     arrived(B.px.at[0:15], B.px_s.at[0])
     arrived(B.zx.at[0:7], B.zx_s.at[0])
     arrived(B.fin.at[0:15], B.fin_s.at[0])
+
+
+def write_out(*refs):
+    ins, outs, sems = refs[:4], refs[4:8], refs[8]
+    copies = [pltpu.make_async_copy(a, b, sems.at[i]) for i, (a, b) in enumerate(zip(ins, outs, strict=True))]
+    for cp in copies:
+        cp.start()
+    for cp in copies:
+        cp.wait()
 
 
 def body(tokens, key_weight, queries, values, cotangent, log_decay):
@@ -515,22 +655,23 @@
         jax.ShapeDtypeStruct((NB, 128, 256), BF16),
         jax.ShapeDtypeStruct((16, 8, WIDTH), F32),
     ]
-    gt, gq, gv, dw = pl.pallas_call(
+    results = pl.pallas_call(
         kernel,
         out_shape=shapes,
-        in_specs=[pl.BlockSpec(memory_space=pltpu.SMEM)] + [hbm] * 7,
+        in_specs=[hbm] * 8,
         out_specs=[vmem] * 4,
         scratch_shapes=[pltpu.VMEM(shape, kind) for shape, kind in SCRATCH.values()]
-        + [pltpu.SemaphoreType.DMA((n,)) for n in SEMS.values()],
+        + [pltpu.SemaphoreType.DMA((n,)) for n in SEMS.values()]
+        + [pltpu.SMEM((16,), F32)],
         compiler_params=pltpu.CompilerParams(
             collective_id=0, has_side_effects=True, vmem_limit_bytes=48 * 2**20
         ),
         name="retention",
     )(
-        log_decay,
         *(
             pltpu.with_memory_space_constraint(a, pltpu.HBM)
             for a in (
+                log_decay,
                 jnp.asarray(inside),
                 jnp.asarray(across),
                 tokens.reshape(256, WIDTH),
@@ -541,6 +682,15 @@
             )
         ),
     )
+    gt, gq, gv, dw = pl.pallas_call(
+        write_out,
+        out_shape=shapes,
+        in_specs=[vmem] * 4,
+        out_specs=[hbm] * 4,
+        scratch_shapes=[pltpu.SemaphoreType.DMA((4,))],
+        compiler_params=pltpu.CompilerParams(vmem_limit_bytes=8 * 2**20),
+        name="write_out",
+    )(*results)
     return (
         gt.reshape(1, 256, WIDTH),
         gq.reshape(1, 4096, 1, 128),

time: 111 us -> 100 us (0.901)
  Pallas kernels: 106 us -> 98.5 us
  local copies, waits for them, and re-layouts: 4.88 us -> 0 us
    pallas_call x1 -> x2, Pallas kernels: 106 us -> 98.5 us  [the longest x1 96.2 us: body(): pl.pallas_call(kernel, out_shape=shapes, in_specs=[hbm] * 8, out_specs=[v...]
    unnamed x6 -> x0, local copies, waits for them, and re-layouts: 4.88 us -> none
where the time goes in v3:
time: 100 us; the launch traced here: 99.2 us
  Pallas kernels  98.5 us (98%)
    pallas_call x1, Pallas kernels, body(): pl.pallas_call(kernel, out_shape=shapes, in_specs=[hbm] * 8, out_specs=[v...  96.2 us
    pallas_call x1, Pallas kernels, body(): pl.pallas_call(write_out, out_shape=shapes, in_specs=[vmem] * 4, out_spec...  2.39 us

profile of v3, /device:TPU:1, one launch (start us, length us, event | category | flops | bytes accessed | tf_op | source)
XLA Modules:
  0.0 99.2 jit_solution(3787690144071565444)
XLA Ops:
  0.6 96.2 %retention.1 = (bf16[256,2048]{1,0:T(8,128)(2,1)S(1)}, bf16[32,128,128]{2,1,0:T(8,128)(2,1)S(1)}, bf16[32,128,256]{2,1,0:T(8,128)(2,1)S(1)}, f32[16,8,2048]{2,1,0:T(8,128)S(1)}) custom-call(f32[16]{0:T(128)} %ld_ref.1, f32[4,128,128]{2,1,0:T(8,128)} %constant.4.clone.jt_ref, f32[32,2,128]{2,1,0:T(2,128)} %constant.5.clone.nt_ref, ...), custom_call_target="tpu_custom_call" | custom-call | tf_op jit(solution)/shard_map/retention/pallas_call | solution.py:658
  96.8 2.4 %write_out.1 = (bf16[256,2048]{1,0:T(8,128)(2,1)}, bf16[32,128,128]{2,1,0:T(8,128)(2,1)}, bf16[32,128,256]{2,1,0:T(8,128)(2,1)}, f32[16,8,2048]{2,1,0:T(8,128)}) custom-call(bf16[256,2048]{1,0:T(8,128)(2,1)S(1)} %get-tuple-element.12.refs_0_, bf16[32,128,128]{2,1,0:T(8,128)(2,1)S(1)} %get-tuple-element.13.refs_1_, ...), custom_call_target="tpu_custom_call" | custom-call | tf_op jit(solution)/shard_map/write_out/pallas_call | solution.py:685

commit v4 on v3

--- a/solution.py
+++ b/solution.py
@@ -17,10 +17,11 @@
 C1 = CHAINS * CW
 C2 = WIDTH - C1
 H2 = C2 // 2
-ORDER = (
-    (1, 1), (3, 3), (3, 1), (1, 3), (2, 1), (2, 3), (1, 2), (3, 2), (2, 2), (1, 0), (3, 0), (0, 2), (2, 0), (0, 1), (0, 3),
-    (0, 0),
-)
+ORDERS = {
+    "cot": ((1, 1), (3, 3), (3, 1), (1, 3), (2, 1), (2, 3), (1, 2), (3, 2), (2, 2), (1, 0), (3, 0), (0, 2), (2, 0), (0, 1), (0, 3), (0, 0)),
+    "gk": ((1, 1), (3, 3), (3, 1), (1, 3), (2, 1), (2, 3), (1, 2), (3, 2), (2, 2), (1, 0), (3, 0), (0, 2), (2, 0), (0, 1), (0, 3), (0, 0)),
+    "end": ((1, 1), (3, 3), (3, 1), (1, 3), (2, 1), (2, 3), (1, 2), (3, 2), (2, 2), (1, 0), (3, 0), (0, 2), (2, 0), (0, 1), (0, 3), (0, 0)),
+}
 FACTOR = BLOCK**-0.5
 
 
@@ -40,11 +41,9 @@
     return lax.dot_general(a, b, (((ca,), (cb,)), ((), ())), preferred_element_type=F32)
 
 
-QUARTERS = (
-    (((2, 0), (2, 1)), ((0, 2), (0, 3))),
-    (((1, 2), (1, 3)), ((3, 0), (3, 1))),
-    (((1, 0), (1, 1)), ((3, 2), (3, 3))),
-    (((0, 0), (0, 1)), ((2, 2), (2, 3))),
+TARGETS = (
+    ((2, 2), (0, 2), (1, 2), (3, 0), (1, 0), (3, 2), (2, 0), (0, 0)),
+    ((2, 1), (0, 3), (1, 3), (3, 1), (1, 1), (3, 3), (2, 3), (0, 1)),
 )
 
 SCRATCH = dict(
@@ -79,15 +78,15 @@
     r1=((2, 2, 4, 8, 8, H2), BF16),
     s1=((2, 4, 8, 8, H2), BF16),
     r2=((2, 4, 8, 8, H2), BF16),
-    zx=((8, 8, C2), BF16),
-    zr=((8, 8, C2), BF16),
+    zx=((2, 8, 8, H2), BF16),
+    zr=((2, 8, 8, H2), BF16),
     px=((16, 8, C1), BF16),
     pr=((16, 8, C1), BF16),
     fin=((16, 8, WIDTH), BF16),
 )
 SEMS = dict(
-    loc=7, cot_s=1, cot_r=16, tok_s=1, tok_r=1, w_s=1, wp_r=7, wm_r=7, gk_s=2, gk_r=1, key_s=2, key_r=1,
-    gt_s=1, gt_r=1, rz_s=1, rz_r=8 * CHAINS, f1_r=4, r1_s=1, r1_r=1, r2_s=1, r2_r=1, zx_s=1, zx_r=1, px_s=1, px_r=1, fin_s=1, finx_r=1, finz_r=1,
+    loc=7, cot_s=1, cot_r=16, tok_s=1, tok_r=1, w_s=1, wp_r=7, wm_r=7, gk_s=2, gk_r=1, key_s=2, key_r=16,
+    gt_s=1, gt_r=1, rz_s=1, rz_r=8 * CHAINS, f1_r=4, r1_s=1, r1_r=2, r2_s=1, r2_r=2, zx_s=1, zx_r=2, px_s=1, px_r=1, fin_s=1, finx_r=2, finz_r=1,
 )
 
 
@@ -99,12 +98,12 @@
     head_core = lax.rem(x, 2)
     head_at = lax.div(sp, 2)
 
-    def plane(t):
+    def plane(t, name="end"):
         if isinstance(t, int):
-            dy, dx = ORDER[t]
+            dy, dx = ORDERS[name][t]
         else:
             code = jnp.int32(0)
-            for k, (a, b) in enumerate(ORDER[:15]):
+            for k, (a, b) in enumerate(ORDERS[name][:15]):
                 code = jnp.where(t == k, a * 4 + b, code)
             dy, dx = lax.div(code, 4), lax.rem(code, 4)
         to = lax.rem(y + dy, 4) * 4 + lax.rem(x + dx, 4)
@@ -184,7 +183,7 @@
             w_copy(0, part, way).start()
 
     def cot_copy(t):
-        to, _ = plane(t)
+        to, _ = plane(t, "cot")
         return remote(
             cot_ref.at[:, :, lanes(to, 256)], B.cot.at[pl.ds(2 * sp, 2)], B.cot_s.at[0], B.cot_r.at[sp], (to, dp)
         )
@@ -232,7 +231,7 @@
             B.keyo.at[hh, pl.ds(2 * i, 2)],
             B.keyi.at[pl.ds(2 * sp, 2)],
             B.key_s.at[sem],
-            B.key_r.at[0],
+            B.key_r.at[sp],
             (2 * hh + c, zdev(0, i)),
         )
 
@@ -245,7 +244,7 @@
             @pl.when(jnp.logical_and(special, own_head_here))
             def _():
                 pltpu.make_async_copy(
-                    B.keyo.at[hh, pl.ds(2 * i, 2)], B.keyi.at[pl.ds(2 * sp, 2)], B.key_r.at[0]
+                    B.keyo.at[hh, pl.ds(2 * i, 2)], B.keyi.at[pl.ds(2 * sp, 2)], B.key_r.at[sp]
                 ).start()
 
             @pl.when(jnp.logical_and(special, jnp.logical_not(own_head_here)))
@@ -257,7 +256,7 @@
                 key_copy(hh, i, 0).start()
 
     def cot_chunk(t):
-        _, p = plane(t)
+        _, p = plane(t, "cot")
         arrived(B.cot.at[pl.ds(2 * p, 2)], B.cot_r.at[p])
         for b in range(2):
             n = 2 * p + b
@@ -287,7 +286,7 @@
         lax.fori_loop(0, NB, scan, jnp.zeros((128, 256), F32))
 
     def gk_copy(t, sem=0):
-        to, _ = plane(t)
+        to, _ = plane(t, "gk")
         return remote(
             B.gko.at[pl.ds(2 * to, 2)],
             B.gki.at[pl.ds(2 * c, 2), :, lanes(head_at)],
@@ -297,7 +296,7 @@
         )
 
     def gk_chunk(t):
-        p, _ = plane(t)
+        p, _ = plane(t, "gk")
         for b in range(2):
             n = 2 * p + b
             g = dot(B.mix[n], B.rq[n], 0, 0) + B.fall[...] * dot(B.vv[n], B.trb[n], 1, 1)
@@ -328,9 +327,9 @@
         for i in range(4):
             B.gkt[:, 128 * i : 128 * i + 128] = B.gki[i].T
 
-    def send_keys(part):
+    def send_keys(lo, hi):
         even = lax.rem(x + c, 2) == 0
-        for (y0, x0), (y1, x1) in QUARTERS[part]:
+        for (y0, x0), (y1, x1) in zip(TARGETS[0][lo:hi], TARGETS[1][lo:hi], strict=True):
             to = lax.rem(y + jnp.where(even, y0, y1), 4) * 4 + lax.rem(x + jnp.where(even, x0, x1), 4)
             key_send(lax.div(to, 2))
 
@@ -399,7 +398,7 @@
             side = 0 if step == 1 else 1
             through, own = pl.ds(2 * side, 2), pl.ds(2 - 2 * side, 2)
             remote(B.dwx.at[way, far, through], B.f1.at[way, side], B.r1_s.at[0], B.f1_r.at[2 * way + side], dev).start()
-            remote(B.dwx.at[way, near, own], B.r1.at[way, side, own], B.r1_s.at[0], B.r1_r.at[0], dev).start()
+            remote(B.dwx.at[way, near, own], B.r1.at[way, side, own], B.r1_s.at[0], B.r1_r.at[way], dev).start()
 
     def line_pass(way):
         for step in (1, 3):
@@ -415,38 +414,36 @@
             loop(0, 8, add)
             through = pl.ds(2 * side, 2)
             remote(
-                B.dwx.at[way, near, through], B.r1.at[way, side, through], B.r1_s.at[0], B.r1_r.at[0], dev
+                B.dwx.at[way, near, through], B.r1.at[way, side, through], B.r1_s.at[0], B.r1_r.at[way], dev
             ).start()
 
-    def line_sums():
-        arrived(B.r1, B.r1_r.at[0])
-        for way, me in ((0, x), (1, y)):
-
-            def add(i):
-                j, hh = lax.div(i, 4), lax.rem(i, 4) * 2
-                total = B.dwx[way, me, j, pl.ds(hh, 2)].astype(F32)
-                for side in range(2):
-                    total += B.r1[way, side, j, pl.ds(hh, 2)].astype(F32)
-                B.s1[way, j, pl.ds(hh, 2)] = total.astype(BF16)
-
-            loop(0, 16, add)
+    def line_sums(way):
+        arrived(B.r1.at[way], B.r1_r.at[way])
+        me = (x, y)[way]
+
+        def add(i):
+            j, hh = lax.div(i, 4), lax.rem(i, 4) * 2
+            total = B.dwx[way, me, j, pl.ds(hh, 2)].astype(F32)
+            for side in range(2):
+                total += B.r1[way, side, j, pl.ds(hh, 2)].astype(F32)
+            B.s1[way, j, pl.ds(hh, 2)] = total.astype(BF16)
+
+        loop(0, 16, add)
         for step in (2, 1, 3):
-            for way in (0, 1):
-                at, me, dev = line(1 - way, step)
-                remote(B.s1.at[way, at], B.r2.at[way, me], B.r2_s.at[0], B.r2_r.at[0], dev).start()
-
-    def plane_sums():
-        arrived(B.r2.at[:, 0:3], B.r2_r.at[0])
-        for way, me in ((0, y), (1, x)):
-            B.r2[way, me] = B.s1[way, me]
-            for hh in range(8):
-                total = B.r2[way, 0, hh].astype(F32)
-                for p in range(1, 4):
-                    total += B.r2[way, p, hh].astype(F32)
-                B.zx[hh, :, way * H2 : way * H2 + H2] = total.astype(BF16)
-        for k in range(1, 8):
+            at, here, dev = line(1 - way, step)
+            remote(B.s1.at[way, at], B.r2.at[way, here], B.r2_s.at[0], B.r2_r.at[way], dev).start()
+
+    def plane_sums(way):
+        arrived(B.r2.at[way, 0:3], B.r2_r.at[way])
+        B.r2[way, (y, x)[way]] = B.s1[way, (y, x)[way]]
+        for hh in range(8):
+            total = B.r2[way, 0, hh].astype(F32)
+            for p in range(1, 4):
+                total += B.r2[way, p, hh].astype(F32)
+            B.zx[way, hh] = total.astype(BF16)
+        for k in (4, 3, 5, 2, 6, 1, 7):
             d = zat(k)
-            remote(B.zx.at[d], B.zr.at[z], B.zx_s.at[0], B.zx_r.at[0], (sp, zdev(k))).start()
+            remote(B.zx.at[way, d], B.zr.at[way, z], B.zx_s.at[0], B.zx_r.at[way], (sp, zdev(k))).start()
 
     def own_rows(i):
         r = pl.ds(pl.multiple_of(i * 16, 16), 16)
@@ -473,11 +470,12 @@
             ref = B.fin.at[sp, :, pl.ds(lo, hi - lo)]
             remote(ref, ref, B.fin_s.at[0], sem, (to, dp)).start()
 
-    def finish_plane_part():
-        arrived(B.zr.at[0:7], B.zx_r.at[0])
-        B.zr[z] = B.zx[z]
-        B.fin[sp, :, C1:WIDTH] = total_of(B.zr, 8)
-        fin_send(C1, WIDTH, B.finx_r.at[0])
+    def finish_plane_part(way):
+        arrived(B.zr.at[way, 0:7], B.zx_r.at[way])
+        B.zr[way, z] = B.zx[way, z]
+        lo = C1 + way * H2
+        B.fin[sp, :, lo : lo + H2] = total_of(B.zr.at[way], 8)
+        fin_send(lo, lo + H2, B.finx_r.at[way])
 
     def finish_ring_part():
         B.pr[sp] = B.px[sp]
@@ -489,7 +487,8 @@
         dw_o[j] = B.fin[j].astype(F32)
 
     def weight_out():
-        arrived(B.fin.at[0:15, :, C1:WIDTH], B.finx_r.at[0])
+        for way in (0, 1):
+            arrived(B.fin.at[0:15, :, C1 + way * H2 : C1 + way * H2 + H2], B.finx_r.at[way])
         arrived(B.fin.at[0:15, :, 0:C1], B.finz_r.at[0])
         loop(0, 16, widen)
 
@@ -517,15 +516,21 @@
             arrived(B.gtr, B.gt_r.at[0])
         loop(lo, hi, gt_tile(False))
 
-    def back_a(i):
-        for b in range(4):
-            n = 4 * i + b
-            u = B.keyi[n].astype(F32)
-            rk = ((u * B.cosv[n] + pltpu.roll(u, 64, 1) * B.sinv[n]) * FACTOR).astype(BF16)
-            B.keyi[n] = rk
-            B.dq[n] = (dot(B.rq[n], rk, 1, 1) * B.within[...]).astype(BF16)
-            dk = (rk.astype(F32) * B.fall[...]).astype(BF16)
-            B.trl[n] = dot(dk, B.vv[n], 0, 0)
+    def back_a(u):
+        for cls in range(2):
+            code = jnp.int32(0)
+            for k, (dy, dx) in enumerate(TARGETS[cls]):
+                code = jnp.where(u == k, (4 - dy) % 4 * 4 + (4 - dx) % 4, code)
+            p = lax.rem(y + lax.div(code, 4), 4) * 4 + lax.rem(x + lax.rem(code, 4), 4)
+            arrived(B.keyi.at[pl.ds(2 * p, 2)], B.key_r.at[p])
+            for b in range(2):
+                n = 2 * p + b
+                k0 = B.keyi[n].astype(F32)
+                rk = ((k0 * B.cosv[n] + pltpu.roll(k0, 64, 1) * B.sinv[n]) * FACTOR).astype(BF16)
+                B.keyi[n] = rk
+                B.dq[n] = (dot(B.rq[n], rk, 1, 1) * B.within[...]).astype(BF16)
+                dk = (rk.astype(F32) * B.fall[...]).astype(BF16)
+                B.trl[n] = dot(dk, B.vv[n], 0, 0)
 
     def scan_up(n, carry):
         B.entb[n] = carry.astype(BF16)
@@ -541,9 +546,6 @@
             for h in range(2):
                 at = slice(128 * h, 128 * h + 128)
                 gv_o[n, :, at] = (near[:, at] + f * far[:, at]).astype(BF16)
-
-    def take_keys():
-        arrived(B.keyi, B.key_r.at[0])
 
     def scores(lo, hi):
         loop(lo, hi, back_a)
@@ -580,36 +582,44 @@
         (weight_ring, 2, 3),
         (w_step, 4, 0),
         (keys_of, 4, 1, 1),
-        (token_grads_partner, 0, 3),
+        (token_grads_partner, 0, 5),
         (take, 0, 4),
+        (line_pass, 0),
         (take, 1, 4),
-        (line_pass, 0),
-        (token_grads_partner, 3, 5),
+        (line_pass, 1),
         (take, 2, 4),
-        (line_pass, 1),
-        (send_keys, 0),
-        (send_keys, 1),
+        (send_keys, 0, 1),
+        (send_keys, 1, 2),
         (token_grads_partner, 5, 8),
         (take, 0, 3),
         (take, 1, 3),
         (take, 2, 3),
-        (line_sums,),
-        (send_keys, 2),
+        (line_sums, 0),
+        (send_keys, 2, 3),
+        (send_keys, 3, 4),
         (take, 0, 2),
         (take, 1, 2),
-        (token_grads, 0, 4),
         (take, 2, 2),
-        (token_grads, 4, 8),
+        (line_sums, 1),
+        (send_keys, 4, 5),
+        (send_keys, 5, 6),
         (take, 0, 1),
+        (token_grads, 0, 3),
         (take, 1, 1),
         (take, 2, 1),
         (column_sums,),
-        (send_keys, 3),
-        (plane_sums,),
+        (send_keys, 6, 7),
+        (send_keys, 7, 8),
+        (scores, 0, 2),
+        (plane_sums, 0),
+        (scores, 2, 3),
+        (plane_sums, 1),
+        (token_grads, 3, 8),
+        (scores, 3, 5),
+        (finish_plane_part, 0),
+        (finish_plane_part, 1),
         (finish_ring_part,),
-        (finish_plane_part,),
-        (take_keys,),
-        (scores, 0, 8),
+        (scores, 5, 8),
         (states,),
         (query_value_grads, 0, 8),
         (weight_out,),
@@ -633,7 +643,7 @@
     arrived(B.dwx.at[:, 0:3], B.r1_s.at[0])
     arrived(B.s1.at[:, 0:3], B.r2_s.at[0])
     arrived(B.px.at[0:15], B.px_s.at[0])
-    arrived(B.zx.at[0:7], B.zx_s.at[0])
+    arrived(B.zx.at[:, 0:7], B.zx_s.at[0])
     arrived(B.fin.at[0:15], B.fin_s.at[0])
 
 

time: 100 us -> 98.2 us (0.982)
  Pallas kernels: 98.5 us -> 96.6 us
    pallas_call x1, Pallas kernels: 96.2 us -> 94.2 us  [body(): pl.pallas_call(kernel, out_shape=shapes, in_specs=[hbm] * 8, out_specs=[v...]
where the time goes in v4:
time: 98.2 us; the launch traced here: 97.2 us
  Pallas kernels  96.6 us (98%)
    pallas_call x1, Pallas kernels, body(): pl.pallas_call(kernel, out_shape=shapes, in_specs=[hbm] * 8, out_specs=[v...  94.2 us
    pallas_call x1, Pallas kernels, body(): pl.pallas_call(write_out, out_shape=shapes, in_specs=[vmem] * 4, out_spec...  2.39 us

profile of v4, /device:TPU:1, one launch (start us, length us, event | category | flops | bytes accessed | tf_op | source)
XLA Modules:
  0.0 97.2 jit_solution(10395259566763371046)
XLA Ops:
  0.6 94.2 %retention.1 = (bf16[256,2048]{1,0:T(8,128)(2,1)S(1)}, bf16[32,128,128]{2,1,0:T(8,128)(2,1)S(1)}, bf16[32,128,256]{2,1,0:T(8,128)(2,1)S(1)}, f32[16,8,2048]{2,1,0:T(8,128)S(1)}) custom-call(f32[16]{0:T(128)} %ld_ref.1, f32[4,128,128]{2,1,0:T(8,128)} %constant.4.clone.jt_ref, f32[32,2,128]{2,1,0:T(2,128)} %constant.5.clone.nt_ref, ...), custom_call_target="tpu_custom_call" | custom-call | tf_op jit(solution)/shard_map/retention/pallas_call | solution.py:668
  94.8 2.4 %write_out.1 = (bf16[256,2048]{1,0:T(8,128)(2,1)}, bf16[32,128,128]{2,1,0:T(8,128)(2,1)}, bf16[32,128,256]{2,1,0:T(8,128)(2,1)}, f32[16,8,2048]{2,1,0:T(8,128)}) custom-call(bf16[256,2048]{1,0:T(8,128)(2,1)S(1)} %get-tuple-element.12.refs_0_, bf16[32,128,128]{2,1,0:T(8,128)(2,1)S(1)} %get-tuple-element.13.refs_1_, ...), custom_call_target="tpu_custom_call" | custom-call | tf_op jit(solution)/shard_map/write_out/pallas_call | solution.py:695

commit v5 on v4

--- a/solution.py
+++ b/solution.py
@@ -614,13 +614,15 @@
         (plane_sums, 0),
         (scores, 2, 3),
         (plane_sums, 1),
-        (token_grads, 3, 8),
-        (scores, 3, 5),
+        (token_grads, 3, 6),
+        (finish_ring_part,),
+        (scores, 3, 4),
         (finish_plane_part, 0),
+        (scores, 4, 5),
         (finish_plane_part, 1),
-        (finish_ring_part,),
         (scores, 5, 8),
         (states,),
+        (token_grads, 6, 8),
         (query_value_grads, 0, 8),
         (weight_out,),
     )
@@ -649,7 +651,12 @@
 
 def write_out(*refs):
     ins, outs, sems = refs[:4], refs[4:8], refs[8]
-    copies = [pltpu.make_async_copy(a, b, sems.at[i]) for i, (a, b) in enumerate(zip(ins, outs, strict=True))]
+    copies = []
+    for a, b in zip(ins, outs, strict=True):
+        rows = a.shape[0] // 4
+        for i in range(4):
+            at = pl.ds(i * rows, rows)
+            copies.append(pltpu.make_async_copy(a.at[at], b.at[at], sems.at[len(copies)]))
     for cp in copies:
         cp.start()
     for cp in copies:
@@ -697,7 +704,7 @@
         out_shape=shapes,
         in_specs=[vmem] * 4,
         out_specs=[hbm] * 4,
-        scratch_shapes=[pltpu.SemaphoreType.DMA((4,))],
+        scratch_shapes=[pltpu.SemaphoreType.DMA((16,))],
         compiler_params=pltpu.CompilerParams(vmem_limit_bytes=8 * 2**20),
         name="write_out",
     )(*results)

time: 98.2 us -> 97.6 us (level)
  no operation moved by 1% of the time
where the time goes in v5:
time: 97.6 us; the launch traced here: 96.9 us
  Pallas kernels  96.2 us (99%)
    pallas_call x1, Pallas kernels, body(): pl.pallas_call(kernel, out_shape=shapes, in_specs=[hbm] * 8, out_specs=[v...  93.8 us
    pallas_call x1, Pallas kernels, body(): pl.pallas_call(write_out, out_shape=shapes, in_specs=[vmem] * 4, out_spec...  2.46 us

profile of v5, /device:TPU:1, one launch (start us, length us, event | category | flops | bytes accessed | tf_op | source)
XLA Modules:
  0.0 96.9 jit_solution(1223926450507025479)
XLA Ops:
  0.6 93.8 %retention.1 = (bf16[256,2048]{1,0:T(8,128)(2,1)S(1)}, bf16[32,128,128]{2,1,0:T(8,128)(2,1)S(1)}, bf16[32,128,256]{2,1,0:T(8,128)(2,1)S(1)}, f32[16,8,2048]{2,1,0:T(8,128)S(1)}) custom-call(f32[16]{0:T(128)} %ld_ref.1, f32[4,128,128]{2,1,0:T(8,128)} %constant.4.clone.jt_ref, f32[32,2,128]{2,1,0:T(2,128)} %constant.5.clone.nt_ref, ...), custom_call_target="tpu_custom_call" | custom-call | tf_op jit(solution)/shard_map/retention/pallas_call | solution.py:675
  94.4 2.5 %write_out.1 = (bf16[256,2048]{1,0:T(8,128)(2,1)}, bf16[32,128,128]{2,1,0:T(8,128)(2,1)}, bf16[32,128,256]{2,1,0:T(8,128)(2,1)}, f32[16,8,2048]{2,1,0:T(8,128)}) custom-call(bf16[256,2048]{1,0:T(8,128)(2,1)S(1)} %get-tuple-element.12.refs_0_, bf16[32,128,128]{2,1,0:T(8,128)(2,1)S(1)} %get-tuple-element.13.refs_1_, ...), custom_call_target="tpu_custom_call" | custom-call | tf_op jit(solution)/shard_map/write_out/pallas_call | solution.py:702

commit v6 on v5

--- a/solution.py
+++ b/solution.py
@@ -20,7 +20,7 @@
 ORDERS = {
     "cot": ((1, 1), (3, 3), (3, 1), (1, 3), (2, 1), (2, 3), (1, 2), (3, 2), (2, 2), (1, 0), (3, 0), (0, 2), (2, 0), (0, 1), (0, 3), (0, 0)),
     "gk": ((1, 1), (3, 3), (3, 1), (1, 3), (2, 1), (2, 3), (1, 2), (3, 2), (2, 2), (1, 0), (3, 0), (0, 2), (2, 0), (0, 1), (0, 3), (0, 0)),
-    "end": ((1, 1), (3, 3), (3, 1), (1, 3), (2, 1), (2, 3), (1, 2), (3, 2), (2, 2), (1, 0), (3, 0), (0, 2), (2, 0), (0, 1), (0, 3), (0, 0)),
+    "end": ((2, 2), (1, 2), (3, 2), (2, 1), (2, 3), (0, 2), (1, 1), (1, 3), (3, 1), (3, 3), (2, 0), (0, 1), (0, 3), (1, 0), (3, 0), (0, 0)),
 }
 FACTOR = BLOCK**-0.5
 
@@ -85,7 +85,7 @@
     fin=((16, 8, WIDTH), BF16),
 )
 SEMS = dict(
-    loc=7, cot_s=1, cot_r=16, tok_s=1, tok_r=1, w_s=1, wp_r=7, wm_r=7, gk_s=2, gk_r=1, key_s=2, key_r=16,
+    loc=7, cot_s=1, cot_r=16, tok_s=1, tok_r=1, w_s=1, wp_r=7, wm_r=7, gk_s=2, gk_r=1, key_s=2, key_r=8,
     gt_s=1, gt_r=1, rz_s=1, rz_r=8 * CHAINS, f1_r=4, r1_s=1, r1_r=2, r2_s=1, r2_r=2, zx_s=1, zx_r=2, px_s=1, px_r=1, fin_s=1, finx_r=2, finz_r=1,
 )
 
@@ -226,34 +226,34 @@
 
         loop(0, 2, part)
 
-    def key_copy(hh, i, sem):
+    def key_copy(hh, i, sem, u):
         return remote(
             B.keyo.at[hh, pl.ds(2 * i, 2)],
             B.keyi.at[pl.ds(2 * sp, 2)],
             B.key_s.at[sem],
-            B.key_r.at[sp],
+            B.key_r.at[u],
             (2 * hh + c, zdev(0, i)),
         )
 
     own_head_here = head_core == c
 
-    def key_send(hh):
+    def key_send(hh, u):
         for i in range(2):
             special = jnp.logical_and(hh == head_at, c == i)
 
             @pl.when(jnp.logical_and(special, own_head_here))
             def _():
                 pltpu.make_async_copy(
-                    B.keyo.at[hh, pl.ds(2 * i, 2)], B.keyi.at[pl.ds(2 * sp, 2)], B.key_r.at[sp]
+                    B.keyo.at[hh, pl.ds(2 * i, 2)], B.keyi.at[pl.ds(2 * sp, 2)], B.key_r.at[u]
                 ).start()
 
             @pl.when(jnp.logical_and(special, jnp.logical_not(own_head_here)))
             def _():
-                key_copy(hh, i, 1).start()
+                key_copy(hh, i, 1, u).start()
 
             @pl.when(jnp.logical_not(special))
             def _():
-                key_copy(hh, i, 0).start()
+                key_copy(hh, i, 0, u).start()
 
     def cot_chunk(t):
         _, p = plane(t, "cot")
@@ -329,9 +329,10 @@
 
     def send_keys(lo, hi):
         even = lax.rem(x + c, 2) == 0
-        for (y0, x0), (y1, x1) in zip(TARGETS[0][lo:hi], TARGETS[1][lo:hi], strict=True):
+        for u in range(lo, hi):
+            (y0, x0), (y1, x1) = TARGETS[0][u], TARGETS[1][u]
             to = lax.rem(y + jnp.where(even, y0, y1), 4) * 4 + lax.rem(x + jnp.where(even, x0, x1), 4)
-            key_send(lax.div(to, 2))
+            key_send(lax.div(to, 2), u)
 
     def ring_refs(chain, way, k):
         at = pl.ds(chain * CW, CW)
@@ -517,12 +518,12 @@
         loop(lo, hi, gt_tile(False))
 
     def back_a(u):
+        arrived(B.keyi.at[0:4], B.key_r.at[u])
         for cls in range(2):
             code = jnp.int32(0)
             for k, (dy, dx) in enumerate(TARGETS[cls]):
                 code = jnp.where(u == k, (4 - dy) % 4 * 4 + (4 - dx) % 4, code)
             p = lax.rem(y + lax.div(code, 4), 4) * 4 + lax.rem(x + lax.rem(code, 4), 4)
-            arrived(B.keyi.at[pl.ds(2 * p, 2)], B.key_r.at[p])
             for b in range(2):
                 n = 2 * p + b
                 k0 = B.keyi[n].astype(F32)

time: 97.6 us -> 97.4 us (level)
  no operation moved by 1% of the time
where the time goes in v6:
time: 97.4 us; the launch traced here: 97.3 us
  Pallas kernels  96.6 us (99%)
    pallas_call x1, Pallas kernels, body(): pl.pallas_call(kernel, out_shape=shapes, in_specs=[hbm] * 8, out_specs=[v...  94.2 us
    pallas_call x1, Pallas kernels, body(): pl.pallas_call(write_out, out_shape=shapes, in_specs=[vmem] * 4, out_spec...  2.46 us

profile of v6, /device:TPU:1, one launch (start us, length us, event | category | flops | bytes accessed | tf_op | source)
XLA Modules:
  0.0 97.3 jit_solution(856628468448113065)
XLA Ops:
  0.6 94.2 %retention.1 = (bf16[256,2048]{1,0:T(8,128)(2,1)S(1)}, bf16[32,128,128]{2,1,0:T(8,128)(2,1)S(1)}, bf16[32,128,256]{2,1,0:T(8,128)(2,1)S(1)}, f32[16,8,2048]{2,1,0:T(8,128)S(1)}) custom-call(f32[16]{0:T(128)} %ld_ref.1, f32[4,128,128]{2,1,0:T(8,128)} %constant.4.clone.jt_ref, f32[32,2,128]{2,1,0:T(2,128)} %constant.5.clone.nt_ref, ...), custom_call_target="tpu_custom_call" | custom-call | tf_op jit(solution)/shard_map/retention/pallas_call | solution.py:676
  94.8 2.5 %write_out.1 = (bf16[256,2048]{1,0:T(8,128)(2,1)}, bf16[32,128,128]{2,1,0:T(8,128)(2,1)}, bf16[32,128,256]{2,1,0:T(8,128)(2,1)}, f32[16,8,2048]{2,1,0:T(8,128)}) custom-call(bf16[256,2048]{1,0:T(8,128)(2,1)S(1)} %get-tuple-element.12.refs_0_, bf16[32,128,128]{2,1,0:T(8,128)(2,1)S(1)} %get-tuple-element.13.refs_1_, ...), custom_call_target="tpu_custom_call" | custom-call | tf_op jit(solution)/shard_map/write_out/pallas_call | solution.py:703
